TPU v7x, 128 devices: a whole 4x4x4 slice. The times are simulated.
128 devices in a mesh: ep: 32 (over z, y, core), tp: 4 (over x).
Axes of the slice: x: 4, y: 4, z: 4, core: 2. Of those that a mesh axis runs over, the one named last changes fastest.
Arguments:
- tokens: bfloat16 [24576, 2048], P('ep')
- in_gain: float32 [2048], replicated, may hold values from 0.1 to 1.9
- route_ids: int32 [24576, 2], P('ep'), may hold values from 0 to 31, all different within a row; in each aligned block of 768 rows (0 to 767, 768 to 1535, ...) at most 96 rows name the same one
- route_scores: float32 [24576, 2], P('ep'), may hold values from 0.1 to 1
- gate_weight: bfloat16 [32, 2048, 1024], P('ep', None, 'tp'), may hold values from -0.125 to 0.125
- up_weight: bfloat16 [32, 2048, 1024], P('ep', None, 'tp'), may hold values from -0.125 to 0.125
- down_weight: bfloat16 [32, 1024, 2048], P('ep', 'tp')
- out_gain: float32 [2048], P('tp'), may hold values from 0.1 to 1.9
Outputs:
- mixed: bfloat16 [24576, 2048], P('ep', 'tp')
Inputs may be any that keep to these rules, and one draw needn't show every extreme that they name: `route_ids`: each row names 2 different experts. Among the rows of one index of ep (aligned blocks of 768 rows) no expert is named more than 96 times, a bound that some block reaches.
All inputs are finite; a program needn't handle non-finite values.
Results may differ from a plain program's by a relative error of at most 0.012.
Values may be sent and summed in bfloat16 or wider, within the bound.
A program may use at most 128 MiB of HBM per device.

v0:
```python
import jax
import jax.numpy as jnp
from jax import lax
from jax.sharding import PartitionSpec as P

epsilon = 1e-06


def copy_for_each(value, axis):
    length = lax.axis_size(axis)
    return lax.all_to_all(
        jnp.broadcast_to(value[None], (length, *value.shape)), axis, 0, 0, tiled=True
    )


def taken_together(value, axis):
    return copy_for_each(value, axis).sum(axis=0)


def per_device(
    tokens, in_gain, route_ids, route_scores, gate_weight, up_weight, down_weight, out_gain
):
    count_ep = lax.axis_size("ep")
    count_tp = lax.axis_size("tp")
    local_experts = gate_weight.shape[0]
    experts = count_ep * local_experts
    tok_count, full_width = tokens.shape
    choose_count = route_ids.shape[1]
    capacity = 2 * tok_count * choose_count // experts
    part_width = full_width // count_tp
    as_float = tokens.astype(jnp.float32)
    normed = (
        as_float
        * lax.rsqrt(jnp.mean(as_float * as_float, axis=1, keepdims=True) + epsilon)
        * in_gain
    ).astype(jnp.bfloat16)
    flat_ids = route_ids.reshape(-1)
    one_hot = (flat_ids[:, None] == jnp.arange(experts, dtype=jnp.int32)[None, :]).astype(jnp.int32)
    slot_index = jnp.sum((jnp.cumsum(one_hot, axis=0) - 1) * one_hot, axis=1)
    row_index = jnp.arange(tok_count * choose_count, dtype=jnp.int32) // choose_count
    buffer = jnp.zeros((experts, capacity, full_width), jnp.bfloat16)
    buffer = buffer.at[flat_ids, slot_index].set(normed[row_index])
    buffer = buffer.reshape(count_ep, local_experts, capacity, full_width)
    received = lax.all_to_all(buffer, "ep", split_axis=0, concat_axis=0, tiled=True)
    gate_acts = jnp.einsum(
        "secd,edf->secf", received, gate_weight, preferred_element_type=jnp.float32
    )
    up_acts = jnp.einsum("secd,edf->secf", received, up_weight, preferred_element_type=jnp.float32)
    hidden = (jax.nn.silu(gate_acts) * up_acts).astype(jnp.bfloat16)
    partial_terms = jnp.einsum(
        "secf,efd->secd", hidden, down_weight, preferred_element_type=jnp.float32
    ).astype(jnp.bfloat16)
    summed = (
        lax.psum_scatter(partial_terms, "tp", scatter_dimension=3, tiled=True)
        .astype(jnp.float32)
        .astype(jnp.bfloat16)
    )
    returned = lax.all_to_all(summed, "ep", split_axis=0, concat_axis=0, tiled=True).reshape(
        experts, capacity, part_width
    )
    picked = (
        returned[flat_ids, slot_index]
        .astype(jnp.float32)
        .reshape(tok_count, choose_count, part_width)
    )
    mix_weight = route_scores / jnp.sum(route_scores, axis=1, keepdims=True)
    combined = jnp.sum(mix_weight[:, :, None] * picked, axis=1)
    squares_sum = taken_together(jnp.sum(combined * combined, axis=1), "tp")
    scaled = combined * lax.rsqrt(squares_sum[:, None] / full_width + epsilon) * out_gain
    return scaled.astype(jnp.bfloat16)


def solution(mesh):
    in_specs = (
        P("ep", None),
        P(),
        P("ep", None),
        P("ep", None),
        P("ep", None, "tp"),
        P("ep", None, "tp"),
        P("ep", "tp", None),
        P("tp"),
    )
    out_specs = P("ep", "tp")
    return jax.shard_map(
        per_device, mesh=mesh, in_specs=in_specs, out_specs=out_specs, check_vma=False
    )
```

profile of v0, /device:TPU:1, one launch (start us, length us, event | category | flops | bytes accessed | tf_op | source)
XLA Modules:
  0.0 440.6 jit_solution(12452868296353077085)
XLA Ops:
  6.5 0.0 copy-start
  6.5 0.0 copy-start.7
  6.5 0.0 copy-start.6
  6.5 0.0 reduce-scatter.2.cloned.1.call-start
  6.5 1.0 copy.31
  7.5 0.2 eq.29
  7.7 0.2 eq.25
  8.0 0.0 copy-start.4
  8.0 0.2 reshape.162
  8.2 0.1 fusion.28
  8.3 9.1 %reduce-window.6 = s32[32,12,128]{2,1,0:T(8,128)S(1)} reduce-window(s32[32,12,128]{2,1,0:T(8,128)S(1)} %fusion.25, s32[]{:T(128)} %constant.34.clone.1), window={size=1x1x128 pad=0_0x0_0x127_0}, to_apply=%region_1.0 | reduce-window | flops 6242304 | bytes 393220 | tf_op jit(solution)/shard_map/reduce-window
  17.4 0.1 slice.12
  17.5 0.2 copy.34
  17.7 0.1 copy.35
  17.8 0.0 copy-start.2
  17.8 0.1 add_add_fusion
  18.0 0.1 fusion.27
  18.1 0.0 copy-done.7
  18.1 0.1 multiply_reduce_fusion.2
  18.2 0.0 copy-done.6
  18.2 0.1 and_reduce_fusion
  18.3 2.8 fusion.4
  21.2 0.0 copy-done.4
  21.2 0.0 copy-done.2
  21.2 2.5 fusion.6
  23.7 34.2 %scatter_custom_fusion = bf16[3072,2048]{1,0:T(8,128)(2,1)} fusion(s32[1536]{0:T(1024)S(1)} %broadcast_select_fusion, bf16[768,2048]{1,0:T(8,128)(2,1)} %fusion.6, s32[2048]{0:T(1024)S(1)} %pad_clamp_fusion, bf16[]{:T(256)} %constant.33.clone.1), kind=kCustom, calls=%fused_computation.13 | custom fusion | bytes 12583424
  57.9 0.0 copy-start.8
  57.9 150.4 %all_to_all.16 = bf16[32,1,96,2048]{3,2,1,0:T(8,128)(2,1)S(1)} all-to-all(bf16[32,1,96,2048]{3,2,1,0:T(8,128)(2,1)} %bitcast.84), channel_id=1, replica_groups=mesh['ep'=32,'tp'=4] {'ep'}, dimensions={0} | all-to-all | bytes 25165824 | tf_op jit(solution)/shard_map/all_to_all | solution.py:44
  208.3 0.0 copy-start.1
  208.3 4.5 %copy-done.1 = bf16[32,1,96,2048]{3,2,1,0:T(8,128)(2,1)} copy-done((bf16[32,1,96,2048]{3,2,1,0:T(8,128)(2,1)}, bf16[32,1,96,2048]{3,2,1,0:T(8,128)(2,1)S(1)}, u32[]{:S(2)}) %copy-start.1) | copy-done | bytes 12582936
  212.7 0.0 copy-done.8
  212.7 0.0 copy-start.9
  212.7 5.3 %fusion.2 = f32[32,96,256]{2,1,0:T(8,128)} fusion(bf16[32,1,96,2048]{3,2,1,0:T(8,128)(2,1)S(1)} %all_to_all.16, bf16[1,2048,256]{2,1,0:T(8,128)(2,1)S(1)} %copy-done.8), kind=kOutput, calls=%fused_computation.5 | convolution fusion | flops 3221225472 | bytes 16777216 | tf_op jit(solution)/shard_map/secd,edf->secf/dot_general | solution.py:45
  218.1 0.0 copy-done
  218.1 0.0 copy-done.9
  218.1 18.7 %convert_bitcast_fusion = bf16[32,1,96,2048]{3,2,0,1:T(8,128)(2,1)} fusion(f32[32,96,256]{2,1,0:T(8,128)} %fusion.2, bf16[32,1,96,2048]{3,2,1,0:T(8,128)(2,1)} %copy-done.1, bf16[1,256,2048]{2,1,0:T(8,128)(2,1)S(1)} %copy-done, bf16[1,2048,256]{2,1,0:T(8,128)(2,1)S(1)} %copy-done.9), kind=kOutput, calls=%fused_computation.7 | convolution fusion | flops 6453460992 | bytes 30408704 | tf_op jit(solution)/shard_map/secf,efd->secd/dot_general | solution.py:50
  236.8 0.0 reduce-scatter.2.cloned.1.call-update
  236.8 112.0 %reduce-scatter.2.cloned.1.call-done = bf16[32,1,96,512]{3,2,0,1:T(8,128)(2,1)} async-done(((bf16[32,1,96,2048]{3,2,0,1:T(8,128)(2,1)}), bf16[32,1,96,512]{3,2,0,1:T(8,128)(2,1)}) %reduce-scatter.2.cloned.1.call-update) | async-done | bytes 3145744 | tf_op jit(solution)/shard_map/reduce_scatter | solution.py:54
  348.9 0.0 copy-start.3
  348.9 8.0 %all-to-all-start.1 = ((bf16[32,1,96,512]{3,2,1,0:T(8,128)(2,1)}), bf16[32,1,96,512]{3,2,1,0:T(8,128)(2,1)}, u32[]{:S(2)}, u32[]{:S(2)}) async-start(bf16[32,1,96,512]{3,2,1,0:T(8,128)(2,1)} %bitcast.85), calls=%async_computation.2 | async-start | bytes 6291456 | tf_op jit(solution)/shard_map/all_to_all | solution.py:58
  356.9 0.0 copy-done.3
  356.9 0.2 copy.30
  357.1 39.2 %all-to-all-done.1 = bf16[32,1,96,512]{3,2,1,0:T(8,128)(2,1)} async-done(((bf16[32,1,96,512]{3,2,1,0:T(8,128)(2,1)}), bf16[32,1,96,512]{3,2,1,0:T(8,128)(2,1)}, u32[]{:S(2)}, u32[]{:S(2)}) %all-to-all-start.1) | async-done | bytes 3145760 | tf_op jit(solution)/shard_map/all_to_all | solution.py:58
  396.3 20.3 %gather_fusion = bf16[1536,512]{1,0:T(8,128)(2,1)S(1)} fusion(bf16[32,96,512]{2,1,0:T(8,128)(2,1)} %bitcast.23, s32[1536]{0:T(1024)S(1)} %get-tuple-element.5), kind=kCustom, calls=%fused_computation.1 | custom fusion | bytes 3158016 | tf_op jit(solution)/shard_map/gather | solution.py:62
  416.6 3.3 reshape.176
  419.9 0.0 copy-start.5
  419.9 6.0 %multiply_reduce_fusion = f32[768,512]{1,0:T(8,128)S(1)} fusion(f32[768,2,512]{2,1,0:T(2,128)} %reshape.176, f32[768,2]{1,0:T(8,128)S(1)} %copy.30), kind=kLoop, calls=%fused_computation.23 | loop fusion | flops 1179648 | bytes 4724736 | tf_op jit(solution)/shard_map/reduce_sum | solution.py:67
  425.9 0.2 multiply_reduce_fusion.1
  426.1 6.5 %all_to_all.17 = f32[4,1,768]{2,1,0:T(1,128)S(1)} all-to-all(f32[4,1,768]{2,1,0:T(1,128)S(1)} %broadcast_in_dim.5), channel_id=1, replica_groups=mesh['ep'=32,'tp'=4] {'tp'}, dimensions={0} | all-to-all | bytes 24576 | tf_op jit(solution)/shard_map/all_to_all | solution.py:11
  432.7 0.0 copy-done.5
  432.7 1.1 multiply_convert_fusion
  (11 shorter events, 0.2 us)
Async XLA Ops:
  6.5 211.6 %copy-start = (bf16[1,256,2048]{2,1,0:T(8,128)(2,1)S(1)}, bf16[1,256,2048]{2,1,0:T(8,128)(2,1)}, u32[]{:S(2)}) copy-start(bf16[1,256,2048]{2,1,0:T(8,128)(2,1)} %param.14) | copy-start | bytes 3145732
  6.5 11.6 %copy-start.7 = (s32[2]{0:T(128)S(1)}, s32[2]{0:T(128)}, u32[]{:S(2)}) copy-start(s32[2]{0:T(128)} %constant.46) | copy-start | bytes 28
  6.5 11.7 %copy-start.6 = (s32[2]{0:T(128)S(1)}, s32[2]{0:T(128)}, u32[]{:S(2)}) copy-start(s32[2]{0:T(128)} %constant.49) | copy-start | bytes 28
  6.5 342.3 %reduce-scatter.2.cloned.1.call-start = ((), (), s32[]{:S(2)}) async-start(), calls=%async_computation.4 | async-start | bytes 15728640 | tf_op jit(solution)/shard_map/reduce_scatter | solution.py:54
  8.0 13.2 %copy-start.4 = (f32[2048]{0:T(1024)S(1)}, f32[2048]{0:T(1024)}, u32[]{:S(2)}) copy-start(f32[2048]{0:T(1024)} %param.9) | copy-start | bytes 24580
  17.8 3.4 copy-start.2
  57.9 154.8 %copy-start.8 = (bf16[1,2048,256]{2,1,0:T(8,128)(2,1)S(1)}, bf16[1,2048,256]{2,1,0:T(8,128)(2,1)}, u32[]{:S(2)}) copy-start(bf16[1,2048,256]{2,1,0:T(8,128)(2,1)} %param.12) | copy-start | bytes 3145732
  208.3 4.5 %copy-start.1 = (bf16[32,1,96,2048]{3,2,1,0:T(8,128)(2,1)}, bf16[32,1,96,2048]{3,2,1,0:T(8,128)(2,1)S(1)}, u32[]{:S(2)}) copy-start(bf16[32,1,96,2048]{3,2,1,0:T(8,128)(2,1)S(1)} %all_to_all.16) | copy-start | bytes 37748740
  212.7 5.4 %copy-start.9 = (bf16[1,2048,256]{2,1,0:T(8,128)(2,1)S(1)}, bf16[1,2048,256]{2,1,0:T(8,128)(2,1)}, u32[]{:S(2)}) copy-start(bf16[1,2048,256]{2,1,0:T(8,128)(2,1)} %param.13) | copy-start | bytes 3145732
  348.9 8.0 %copy-start.3 = (f32[768,2]{0,1:T(2,128)S(1)}, f32[768,2]{0,1:T(2,128)}, u32[]{:S(2)}) copy-start(f32[768,2]{0,1:T(2,128)} %param.11) | copy-start | bytes 18436
  348.9 47.4 %all-to-all-start.1 = ((bf16[32,1,96,512]{3,2,1,0:T(8,128)(2,1)}), bf16[32,1,96,512]{3,2,1,0:T(8,128)(2,1)}, u32[]{:S(2)}, u32[]{:S(2)}) async-start(bf16[32,1,96,512]{3,2,1,0:T(8,128)(2,1)} %bitcast.85), calls=%async_computation.2 | async-start | bytes 6291456 | tf_op jit(solution)/shard_map/all_to_all | solution.py:58
  419.9 12.8 %copy-start.5 = (f32[512]{0:T(512)S(1)}, f32[512]{0:T(512)}, u32[]{:S(2)}) copy-start(f32[512]{0:T(512)} %param.15) | copy-start | bytes 6148
Sparse Core Ops, SparseCore 0:
  237.0 111.8 reduce-scatter.1
where the time goes:
time: 444 us; the launch traced here: 441 us
  blocking collectives  157 us (35%)
  waiting for transfers between devices  151 us (34%)
  local copies, waits for them, and re-layouts  64.6 us (15%)
  matrix products  24.1 us (5%)
  other arithmetic  22.2 us (5%)
  between operations  13.6 us (3%)
  starting transfers between devices  7.96 us (2%)
    all_to_all x1, blocking collectives, per_device(): lax.all_to_all(buffer, 'ep', split_axis=0, concat_axis=0, tiled=True)  150 us
    reduce_scatter x1, waiting for transfers between devices, per_device(): lax.psum_scatter(partial_terms, 'tp', scatter_dimension=3, tiled=True)  112 us
    unnamed x22, local copies, waits for them, and re-layouts  39.7 us
    all_to_all x1, waiting for transfers between devices, per_device(): lax.all_to_all(summed, 'ep', split_axis=0, concat_axis=0, tiled=True)  39.2 us
    gather x1, local copies, waits for them, and re-layouts, per_device(): returned[flat_ids, slot_index].astype(jnp.float32)  20.3 us
    dot_general x1, matrix products, per_device(): jnp.einsum('secf,efd->secd', hidden, down_weight, preferred_element_type=...  18.7 us
    another operation x2, other arithmetic  9.11 us
  transfers between devices with their start and end apart: 2, of which 2 were waited for; matrix products, arithmetic and copies ran while one was open for 0% of the time, Pallas kernels for 0%

commit v1 on v0

v1 whole, which is shorter than its diff:
```python
import jax
import jax.numpy as jnp
from jax import lax
from jax.experimental import pallas as pl
from jax.experimental.pallas import tpu as pltpu
from jax.sharding import PartitionSpec as P

EPS = 1e-06
MESH = pl.DeviceIdType.MESH
T = 768
D = 2048
F = 256
CAP = 96
HALF = 48
ROWS = 4 * 2 * HALF
DQ = 512
f32 = jnp.float32
bf16 = jnp.bfloat16


def dot(a, b):
    return jnp.dot(a, b, preferred_element_type=f32)


def at_rows(ref, start, size):
    return ref.at[pl.ds(pl.multiple_of(start, 16), size), :]


def kernel(
    tok_hbm, gain_ref, ids_ref, score_ref, wg_hbm, wu_hbm, wd_hbm, og_ref,
    out_ref,
    tok, s_buf, x_buf, wg, wu, wd, h_buf, h_recv, y_buf, r_buf,
    slot_t, onehot, sel, col0, col1, mix0, mix1, rowsum, comb, ns_buf, ns_recv,
    local_sem, s_send, x_recv, w_send, w_recv, h_send, h_rsem, y_send, r_recv, n_send, n_recv,
):
    ep = lax.axis_index("ep")
    x = lax.axis_index("tp")
    z = ep // 8
    y = (ep // 2) % 4
    c = ep % 2
    xs = (x - c + 5) % 4
    half = xs // 2
    member = xs % 2
    x_gate = ((((x - c + 4) % 4) + 1 - 2 * (((x - c + 4) % 4) % 2)) + c) % 4
    x_hid = (xs + 1 - 2 * member + c + 3) % 4
    x_far = (x + 2) % 4
    dm = (c + member) % 2

    def source_of(g, j, dc, sign):
        dy = (j + g + 1) % 4
        return (
            ((z + sign * j + 4) % 4) * 8 + ((y + sign * dy + 4) % 4) * 2 + (c + dc) % 2
        )

    tok_copy = pltpu.make_async_copy(tok_hbm, tok, local_sem.at[0])
    tok_copy.start()
    wg_copy = pltpu.make_async_copy(wg_hbm, wg.at[0], local_sem.at[1])
    wu_copy = pltpu.make_async_copy(wu_hbm, wu.at[0], local_sem.at[2])
    wd_copy = pltpu.make_async_copy(wd_hbm, wd.at[pl.ds(0, F), :], local_sem.at[3])
    wg_copy.start()
    wu_copy.start()
    wd_copy.start()

    barrier = pltpu.get_barrier_semaphore()

    def greet(i, _):
        d = (ep * 4 + x + i) % 128
        pl.semaphore_signal(barrier, inc=1, device_id=(d // 4, d % 4), device_id_type=MESH)
        return 0

    lax.fori_loop(1, 128, greet, 0)

    lanes = lax.broadcasted_iota(jnp.int32, (128, 128), 1)
    dz_l = ((lanes >> 3) - z) & 3
    dy_l = (((lanes >> 1) & 3) - y) & 3
    dc_l = ((lanes & 1) - c) & 1
    base = ((((dy_l - dz_l + 3) & 3) * 8 + dc_l * 4 + dz_l) * CAP).astype(f32)

    def mark(b, _):
        rows = pl.ds(pl.multiple_of(b * 128, 128), 128)
        ids = ids_ref[rows, :]
        named = (ids[:, 0:1] == lanes) | (ids[:, 1:2] == lanes)
        onehot[rows, :] = jnp.where(named, 1.0, 0.0).astype(bf16)
        return 0

    lax.fori_loop(0, 6, mark, 0)

    def number(b, _):
        rows = pl.ds(pl.multiple_of(b * 128, 128), 128)
        earlier = lax.broadcasted_iota(jnp.int32, (128, T), 1) < (
            lax.broadcasted_iota(jnp.int32, (128, T), 0) + b * 128
        )
        count = dot(jnp.where(earlier, 1.0, 0.0).astype(bf16), onehot[...])
        ids = ids_ref[rows, :]
        first = ids[:, 0:1] == lanes
        second = ids[:, 1:2] == lanes
        slot_t[:, rows] = jnp.where(first | second, count, -1.0).T
        place = count + base
        score = score_ref[rows, :]
        total = score[:, 0:1] + score[:, 1:2]
        col0[rows, :] = jnp.broadcast_to(
            jnp.sum(jnp.where(first, place, 0.0), axis=1, keepdims=True), (128, 128)
        )
        col1[rows, :] = jnp.broadcast_to(
            jnp.sum(jnp.where(second, place, 0.0), axis=1, keepdims=True), (128, 128)
        )
        mix0[rows, :] = jnp.broadcast_to(score[:, 0:1] / total, (128, 128))
        mix1[rows, :] = jnp.broadcast_to(score[:, 1:2] / total, (128, 128))
        return 0

    lax.fori_loop(0, 6, number, 0)

    tok_copy.wait()

    def squares(b, _):
        rows = pl.ds(pl.multiple_of(b * 64, 64), 64)
        acc = jnp.zeros((64, 128), f32)
        for q in range(16):
            v = tok[rows, q * 128 : (q + 1) * 128].astype(f32)
            acc = acc + v * v
        rowsum[rows, :] = acc
        return 0

    lax.fori_loop(0, 12, squares, 0)

    def scale_of(b, _):
        rows = pl.ds(pl.multiple_of(b * 256, 256), 256)
        mean = jnp.sum(rowsum[rows, :], axis=1, keepdims=True) * (1.0 / D)
        rowsum[rows, :] = jnp.broadcast_to(lax.rsqrt(mean + EPS), (256, 128))
        return 0

    lax.fori_loop(0, 3, scale_of, 0)

    def normalize(b, _):
        rows = pl.ds(pl.multiple_of(b * 64, 64), 64)
        scale = rowsum[rows, :]
        for q in range(16):
            cols = slice(q * 128, (q + 1) * 128)
            v = tok[rows, cols].astype(f32) * scale * gain_ref[:, cols]
            tok[rows, cols] = v.astype(bf16)
        return 0

    lax.fori_loop(0, 12, normalize, 0)

    def pack(g, _):
        for q in range(8):
            dc, j = q // 4, q % 4
            e = source_of(g, j, dc, 1)
            first = ((x - (c + dc) % 2 + 5) % 4) // 2 * HALF
            want = lax.broadcasted_iota(jnp.int32, (HALF, T), 0) + first
            row = slot_t[pl.ds(e, 1), :]
            sel[q * HALF : (q + 1) * HALF, :] = jnp.where(
                row == want.astype(f32), 1.0, 0.0
            ).astype(bf16)
        rows = pl.ds(pl.multiple_of(g * ROWS, ROWS), ROWS)

        def part(n, _):
            cols = pl.ds(pl.multiple_of(n * 512, 512), 512)
            s_buf[rows, cols] = dot(sel[0:ROWS, :], tok[:, cols]).astype(bf16)
            return 0

        lax.fori_loop(0, 4, part, 0)
        return 0

    lax.fori_loop(0, 4, pack, 0)
    own = slice(24 * HALF, 25 * HALF)
    x_buf[own, :] = s_buf[own, :]

    pl.semaphore_wait(barrier, 127)

    def send_weight(src, dst, to, sem):
        cp = pltpu.make_async_remote_copy(
            src_ref=src, dst_ref=dst, send_sem=w_send.at[sem], recv_sem=w_recv.at[sem],
            device_id=(ep, to), device_id_type=MESH,
        )
        cp.start()
        return cp

    w_copies = [
        send_weight(wg_hbm, wg.at[1], x_gate, 0),
        send_weight(wu_hbm, wu.at[1], x_gate, 1),
        send_weight(wd_hbm, wd.at[pl.ds(2 * F, F), :], x_hid, 2),
        send_weight(wd_hbm, wd.at[pl.ds(F, F), :], x_gate, 3),
        send_weight(wd_hbm, wd.at[pl.ds(3 * F, F), :], x_far, 4),
    ]

    def dispatch(g, _):
        def one(q, _):
            k, dc, j = q // 8, (q // 4) % 2, q % 4

            @pl.when(jnp.logical_or(g < 3, q % 8 > 0))
            def _():
                row = (g * 8 + q % 8) * HALF + k * 16
                pltpu.make_async_remote_copy(
                    src_ref=at_rows(s_buf, row, 16), dst_ref=at_rows(x_buf, row, 16),
                    send_sem=s_send, recv_sem=x_recv.at[g],
                    device_id=(source_of(g, j, dc, 1), x), device_id_type=MESH,
                ).start()

            return 0

        lax.fori_loop(0, 24, one, 0)
        return 0

    lax.fori_loop(0, 4, dispatch, 0)

    def arrived(ref, rows, sem):
        part = ref.at[pl.ds(0, rows), :]
        pltpu.make_async_copy(part, part, sem).wait()

    wg_copy.wait()
    wu_copy.wait()
    wd_copy.wait()
    for cp in w_copies[:2]:
        cp.wait()

    def expert(g, _):
        @pl.when(g < 3)
        def _():
            arrived(x_buf, ROWS, x_recv.at[g])

        @pl.when(g == 3)
        def _():
            arrived(x_buf, ROWS - HALF, x_recv.at[g])

        rows = pl.ds(pl.multiple_of(g * ROWS, ROWS), ROWS)
        for k in range(2):
            gate = dot(x_buf[rows, :], wg[k])
            up = dot(x_buf[rows, :], wu[k])
            hid = (gate / (1.0 + jnp.exp(-gate)) * up).astype(bf16)
            h_buf[g * 2, :, k * F : (k + 1) * F] = hid[: ROWS // 2]
            h_buf[g * 2 + 1, :, k * F : (k + 1) * F] = hid[ROWS // 2 :]
        cp = pltpu.make_async_remote_copy(
            src_ref=h_buf.at[g * 2 + 1 - dm], dst_ref=h_recv.at[g],
            send_sem=h_send.at[g], recv_sem=h_rsem.at[g],
            device_id=(ep, x_hid), device_id_type=MESH,
        )
        cp.start()

        @pl.when(g == 0)
        def _():
            for late in w_copies[2:]:
                late.wait()

        cp.wait()

        def down(q, _):
            cols = pl.ds(pl.multiple_of(q * DQ, DQ), DQ)
            v = dot(h_buf[g * 2 + dm], wd[0 : 2 * F, cols])
            v = v + dot(h_recv[g], wd[2 * F : 4 * F, cols])
            y_buf[pl.ds(pl.multiple_of((g * 4 + q) * ROWS // 2, ROWS // 2), ROWS // 2), :] = (
                v.astype(bf16)
            )
            return 0

        lax.fori_loop(0, 4, down, 0)

        def give(q, _):
            j = q % 4
            to = (x + q // 4 + j) % 4
            src = ((g * 4 + to) * 4 + j) * HALF
            dst = ((g * 8 + dm * 4 + j) * 2 + half) * HALF
            mine = (g == 3) & (j == 0) & (dm == 0) & (to == x)

            @pl.when(jnp.logical_not(mine))
            def _():
                pltpu.make_async_remote_copy(
                    src_ref=at_rows(y_buf, src, HALF), dst_ref=at_rows(r_buf, dst, HALF),
                    send_sem=y_send, recv_sem=r_recv.at[g],
                    device_id=(source_of(g, j, dm, -1), to), device_id_type=MESH,
                ).start()

            return 0

        lax.fori_loop(0, 16, give, 0)
        return 0

    lax.fori_loop(0, 4, expert, 0)

    @pl.when(dm == 0)
    def _():
        src = pl.ds(pl.multiple_of((12 + x) * 4 * HALF, 16), HALF)
        dst = pl.ds(pl.multiple_of((48 + half) * HALF, 16), HALF)
        r_buf[dst, :] = y_buf[src, :]

    comb[...] = jnp.zeros_like(comb)

    def combine(g, _):
        def weigh(b, _):
            rows = pl.ds(pl.multiple_of(b * 128, 128), 128)
            for q in range(6):
                here = (lanes + (g * 8 * CAP + q * 128)).astype(f32)
                v = jnp.where(col0[rows, :] == here, mix0[rows, :], 0.0)
                v = v + jnp.where(col1[rows, :] == here, mix1[rows, :], 0.0)
                sel[rows, q * 128 : (q + 1) * 128] = v.astype(bf16)
            return 0

        lax.fori_loop(0, 6, weigh, 0)

        @pl.when(jnp.logical_or(g < 3, dm == 1))
        def _():
            arrived(r_buf, 16 * HALF, r_recv.at[g])

        @pl.when(jnp.logical_and(g == 3, dm == 0))
        def _():
            arrived(r_buf, 15 * HALF, r_recv.at[g])

        rows = pl.ds(pl.multiple_of(g * 8 * CAP, 8 * CAP), 8 * CAP)
        comb[...] += dot(sel[...], r_buf[rows, :])
        return 0

    lax.fori_loop(0, 4, combine, 0)

    def square_sum(b, _):
        rows = pl.ds(pl.multiple_of(b * 128, 128), 128)
        acc = jnp.zeros((128, 128), f32)
        for q in range(4):
            v = comb[rows, q * 128 : (q + 1) * 128]
            acc = acc + v * v
        ns_buf[:, rows] = jnp.sum(acc.T.reshape(16, 8, 128), axis=0)
        return 0

    lax.fori_loop(0, 6, square_sum, 0)
    n_copies = []
    for d in range(1, 4):
        cp = pltpu.make_async_remote_copy(
            src_ref=ns_buf, dst_ref=ns_recv.at[d - 1], send_sem=n_send.at[d - 1],
            recv_sem=n_recv.at[d - 1], device_id=(ep, (x + d) % 4), device_id_type=MESH,
        )
        cp.start()
        n_copies.append(cp)
    for cp in n_copies:
        cp.wait()

    def finish(b, _):
        rows = pl.ds(pl.multiple_of(b * 128, 128), 128)
        total = ns_buf[:, rows] + ns_recv[0, :, rows] + ns_recv[1, :, rows] + ns_recv[2, :, rows]
        total = jnp.sum(total, axis=0, keepdims=True)
        scale = lax.rsqrt(total * (1.0 / D) + EPS)
        scale = jnp.broadcast_to(scale, (128, 128)).T
        for q in range(4):
            cols = slice(q * 128, (q + 1) * 128)
            out_ref[rows, cols] = (comb[rows, cols] * scale * og_ref[:, cols]).astype(bf16)
        return 0

    lax.fori_loop(0, 6, finish, 0)

    arrived(s_buf, 31 * HALF, s_send)

    @pl.when(dm == 0)
    def _():
        arrived(y_buf, 63 * HALF, y_send)

    @pl.when(dm == 1)
    def _():
        arrived(y_buf, 64 * HALF, y_send)


def per_device(
    tokens, in_gain, route_ids, route_scores, gate_weight, up_weight, down_weight, out_gain
):
    vmem = pl.BlockSpec(memory_space=pltpu.VMEM)
    hbm = pl.BlockSpec(memory_space=pl.ANY)
    dma = pltpu.SemaphoreType.DMA
    return pl.pallas_call(
        kernel,
        out_shape=jax.ShapeDtypeStruct((T, DQ), bf16),
        in_specs=[hbm, vmem, vmem, vmem, hbm, hbm, hbm, vmem],
        out_specs=vmem,
        scratch_shapes=[
            pltpu.VMEM((T, D), bf16),
            pltpu.VMEM((4 * ROWS, D), bf16),
            pltpu.VMEM((4 * ROWS, D), bf16),
            pltpu.VMEM((2, D, F), bf16),
            pltpu.VMEM((2, D, F), bf16),
            pltpu.VMEM((4 * F, D), bf16),
            pltpu.VMEM((8, ROWS // 2, 2 * F), bf16),
            pltpu.VMEM((4, ROWS // 2, 2 * F), bf16),
            pltpu.VMEM((64 * HALF, DQ), bf16),
            pltpu.VMEM((64 * HALF, DQ), bf16),
            pltpu.VMEM((128, T), f32),
            pltpu.VMEM((T, 128), bf16),
            pltpu.VMEM((T, T), bf16),
            pltpu.VMEM((T, 128), f32),
            pltpu.VMEM((T, 128), f32),
            pltpu.VMEM((T, 128), f32),
            pltpu.VMEM((T, 128), f32),
            pltpu.VMEM((T, 128), f32),
            pltpu.VMEM((T, DQ), f32),
            pltpu.VMEM((8, T), f32),
            pltpu.VMEM((3, 8, T), f32),
            dma((4,)),
            dma,
            dma((4,)),
            dma((5,)),
            dma((5,)),
            dma((4,)),
            dma((4,)),
            dma,
            dma((4,)),
            dma((3,)),
            dma((3,)),
        ],
        compiler_params=pltpu.CompilerParams(
            collective_id=0, has_side_effects=True, vmem_limit_bytes=62 * 2**20
        ),
        name="routed_experts",
    )(
        tokens,
        in_gain.reshape(1, D),
        route_ids,
        route_scores,
        gate_weight.reshape(D, F),
        up_weight.reshape(D, F),
        down_weight.reshape(F, D),
        out_gain.reshape(1, DQ),
    )


def solution(mesh):
    in_specs = (
        P("ep", None),
        P(),
        P("ep", None),
        P("ep", None),
        P("ep", None, "tp"),
        P("ep", None, "tp"),
        P("ep", "tp", None),
        P("tp"),
    )
    return jax.shard_map(
        per_device, mesh=mesh, in_specs=in_specs, out_specs=P("ep", "tp"), check_vma=False
    )
```

time: 444 us -> 165 us (0.37)
  Pallas kernels: 0 us -> 159 us
  blocking collectives: 157 us -> 0 us
  waiting for transfers between devices: 151 us -> 0 us
  local copies, waits for them, and re-layouts: 64.6 us -> 5.31 us
  matrix products: 24.1 us -> 0 us
  other arithmetic: 22.2 us -> 0 us
  between operations: 13.6 us -> 0.01 us
  starting transfers between devices: 7.96 us -> 0 us
    pallas_call x0 -> x1, Pallas kernels: none -> 159 us  [per_device(): pl.pallas_call(kernel, out_shape=jax.ShapeDtypeStruct((T, DQ), bf16), in_...]
    all_to_all x2 -> x0, blocking collectives: 157 us -> none  [the longest x1 150 us: per_device(): lax.all_to_all(buffer, 'ep', split_axis=0, concat_axis=0, tiled=True)]
    reduce_scatter x1 -> x0, waiting for transfers between devices: 112 us -> none  [per_device(): lax.psum_scatter(partial_terms, 'tp', scatter_dimension=3, tiled=True)]
    all_to_all x1 -> x0, waiting for transfers between devices: 39.2 us -> none  [per_device(): lax.all_to_all(summed, 'ep', split_axis=0, concat_axis=0, tiled=True)]
    unnamed x22 -> x3, local copies, waits for them, and re-layouts: 39.7 us -> 5.31 us
    dot_general x2 -> x0, matrix products: 24.1 us -> none  [the longest x1 18.7 us: per_device(): jnp.einsum('secf,efd->secd', hidden, down_weight, preferred_element_type=...]
    gather x1 -> x0, local copies, waits for them, and re-layouts: 20.3 us -> none  [per_device(): returned[flat_ids, slot_index].astype(jnp.float32)]
    reduce_sum x6 -> x0, other arithmetic: 9.11 us -> none  [the longest x1 6 us: per_device(): combined = jnp.sum(mix_weight[:, :, None] * picked, axis=1)]
  transfers between devices with their start and end apart: 2 -> 0, of which waited for: 2 -> 0; matrix products, arithmetic and copies ran while one was open for 0% -> 0% of each run, Pallas kernels for 0% -> 0%
where the time goes in v1:
time: 165 us
  Pallas kernels  159 us (96%)
  local copies, waits for them, and re-layouts  5.31 us (3%)
    pallas_call x1, Pallas kernels, per_device(): pl.pallas_call(kernel, out_shape=jax.ShapeDtypeStruct((T, DQ), bf16), in_...  159 us
    unnamed x3, local copies, waits for them, and re-layouts  5.31 us

profile of v1, /device:TPU:1, one launch (start us, length us, event | category | flops | bytes accessed | tf_op | source)
XLA Modules:
  0.0 164.8 jit_solution(11687103105284719783)
XLA Ops:
  0.0 1.6 copy.9.ids_ref
  1.6 1.6 copy.10.score_ref
  3.2 159.5 %routed_experts.1 = bf16[768,512]{1,0:T(8,128)(2,1)} custom-call(bf16[768,2048]{1,0:T(8,128)(2,1)} %tok_hbm.1, f32[1,2048]{1,0:T(1,128)} %bitcast.8, s32[768,2]{1,0:T(8,128)} %copy.9.ids_ref, f32[768,2]{1,0:T(8,128)} %copy.10.score_ref, bf16[2048,256]{1,0:T(8,128)(2,1)} %bitcast.5, bf16[2048,256]{1,0:T(8,128)(2,1)} %bitcast.6, bf16[256,2048]{1,0:T(8,128)(2,1)} %bitcast.7, ...), custom_call_target="tpu_custom_call" | custom-call | tf_op jit(solution)/shard_map/routed_experts/pallas_call | solution.py:365
  162.7 2.1 %copy.12 = bf16[768,512]{1,0:T(8,128)(2,1)} copy(bf16[768,512]{1,0:T(8,128)(2,1)} %routed_experts.1) | data formatting | bytes 1572864

commit v2 on v1

--- a/solution.py
+++ b/solution.py
@@ -31,7 +31,7 @@
     out_ref,
     tok, s_buf, x_buf, wg, wu, wd, h_buf, h_recv, y_buf, r_buf,
     slot_t, onehot, sel, col0, col1, mix0, mix1, rowsum, comb, ns_buf, ns_recv,
-    local_sem, s_send, x_recv, w_send, w_recv, h_send, h_rsem, y_send, r_recv, n_send, n_recv,
+    local_sem, s_send, x_recv, w_send, w_recv, h_send, h_rsem, y_send, r_recv, n_send, n_recv, ready,
 ):
     ep = lax.axis_index("ep")
     x = lax.axis_index("tp")
@@ -64,11 +64,16 @@
     barrier = pltpu.get_barrier_semaphore()
 
     def greet(i, _):
-        d = (ep * 4 + x + i) % 128
-        pl.semaphore_signal(barrier, inc=1, device_id=(d // 4, d % 4), device_id_type=MESH)
-        return 0
-
-    lax.fori_loop(1, 128, greet, 0)
+        pl.semaphore_signal(
+            barrier, inc=1, device_id=((ep + i) % 32, x), device_id_type=MESH
+        )
+        return 0
+
+    lax.fori_loop(1, 32, greet, 0)
+    for d in range(1, 4):
+        pl.semaphore_signal(
+            barrier, inc=1, device_id=(ep, (x + d) % 4), device_id_type=MESH
+        )
 
     lanes = lax.broadcasted_iota(jnp.int32, (128, 128), 1)
     dz_l = ((lanes >> 3) - z) & 3
@@ -76,11 +81,23 @@
     dc_l = ((lanes & 1) - c) & 1
     base = ((((dy_l - dz_l + 3) & 3) * 8 + dc_l * 4 + dz_l) * CAP).astype(f32)
 
+    lanes_f = lanes.astype(f32)
+
+    def column(row):
+        return jnp.broadcast_to(row, (128, 128)).T
+
     def mark(b, _):
         rows = pl.ds(pl.multiple_of(b * 128, 128), 128)
-        ids = ids_ref[rows, :]
-        named = (ids[:, 0:1] == lanes) | (ids[:, 1:2] == lanes)
+        first = column(ids_ref[0:1, rows].astype(f32))
+        second = column(ids_ref[1:2, rows].astype(f32))
+        col0[rows, :] = first
+        col1[rows, :] = second
+        named = (first == lanes_f) | (second == lanes_f)
         onehot[rows, :] = jnp.where(named, 1.0, 0.0).astype(bf16)
+        score0 = score_ref[0:1, rows]
+        score1 = score_ref[1:2, rows]
+        mix0[rows, :] = column(score0 / (score0 + score1))
+        mix1[rows, :] = column(score1 / (score0 + score1))
         return 0
 
     lax.fori_loop(0, 6, mark, 0)
@@ -91,21 +108,16 @@
             lax.broadcasted_iota(jnp.int32, (128, T), 0) + b * 128
         )
         count = dot(jnp.where(earlier, 1.0, 0.0).astype(bf16), onehot[...])
-        ids = ids_ref[rows, :]
-        first = ids[:, 0:1] == lanes
-        second = ids[:, 1:2] == lanes
+        first = col0[rows, :] == lanes_f
+        second = col1[rows, :] == lanes_f
         slot_t[:, rows] = jnp.where(first | second, count, -1.0).T
         place = count + base
-        score = score_ref[rows, :]
-        total = score[:, 0:1] + score[:, 1:2]
         col0[rows, :] = jnp.broadcast_to(
             jnp.sum(jnp.where(first, place, 0.0), axis=1, keepdims=True), (128, 128)
         )
         col1[rows, :] = jnp.broadcast_to(
             jnp.sum(jnp.where(second, place, 0.0), axis=1, keepdims=True), (128, 128)
         )
-        mix0[rows, :] = jnp.broadcast_to(score[:, 0:1] / total, (128, 128))
-        mix1[rows, :] = jnp.broadcast_to(score[:, 1:2] / total, (128, 128))
         return 0
 
     lax.fori_loop(0, 6, number, 0)
@@ -162,28 +174,6 @@
         lax.fori_loop(0, 4, part, 0)
         return 0
 
-    lax.fori_loop(0, 4, pack, 0)
-    own = slice(24 * HALF, 25 * HALF)
-    x_buf[own, :] = s_buf[own, :]
-
-    pl.semaphore_wait(barrier, 127)
-
-    def send_weight(src, dst, to, sem):
-        cp = pltpu.make_async_remote_copy(
-            src_ref=src, dst_ref=dst, send_sem=w_send.at[sem], recv_sem=w_recv.at[sem],
-            device_id=(ep, to), device_id_type=MESH,
-        )
-        cp.start()
-        return cp
-
-    w_copies = [
-        send_weight(wg_hbm, wg.at[1], x_gate, 0),
-        send_weight(wu_hbm, wu.at[1], x_gate, 1),
-        send_weight(wd_hbm, wd.at[pl.ds(2 * F, F), :], x_hid, 2),
-        send_weight(wd_hbm, wd.at[pl.ds(F, F), :], x_gate, 3),
-        send_weight(wd_hbm, wd.at[pl.ds(3 * F, F), :], x_far, 4),
-    ]
-
     def dispatch(g, _):
         def one(q, _):
             k, dc, j = q // 8, (q // 4) % 2, q % 4
@@ -202,7 +192,39 @@
         lax.fori_loop(0, 24, one, 0)
         return 0
 
-    lax.fori_loop(0, 4, dispatch, 0)
+    def send_weight(src, dst, to, sem):
+        cp = pltpu.make_async_remote_copy(
+            src_ref=src, dst_ref=dst, send_sem=w_send.at[sem], recv_sem=w_recv.at[sem],
+            device_id=(ep, to), device_id_type=MESH,
+        )
+        cp.start()
+        return cp
+
+    def shard(k, lo=0, size=F):
+        return wd.at[pl.ds(k * F + lo, size), :]
+
+    pack(0, 0)
+    pl.semaphore_wait(barrier, 34)
+    w_copies = [
+        send_weight(wg_hbm, wg.at[1], x_gate, 0),
+        send_weight(wu_hbm, wu.at[1], x_gate, 1),
+        send_weight(wd_hbm, shard(2), x_hid, 2),
+        send_weight(wd_hbm, shard(1), x_gate, 3),
+    ]
+    dispatch(0, 0)
+    for d in range(1, 4):
+        pl.semaphore_signal(
+            ready, inc=1, device_id=(ep, (x + d) % 4), device_id_type=MESH
+        )
+
+    def pack_and_send(g, _):
+        pack(g, 0)
+        dispatch(g, 0)
+        return 0
+
+    lax.fori_loop(1, 4, pack_and_send, 0)
+    own = slice(24 * HALF, 25 * HALF)
+    x_buf[own, :] = s_buf[own, :]
 
     def arrived(ref, rows, sem):
         part = ref.at[pl.ds(0, rows), :]
@@ -214,37 +236,29 @@
     for cp in w_copies[:2]:
         cp.wait()
 
-    def expert(g, _):
-        @pl.when(g < 3)
-        def _():
-            arrived(x_buf, ROWS, x_recv.at[g])
-
-        @pl.when(g == 3)
-        def _():
-            arrived(x_buf, ROWS - HALF, x_recv.at[g])
-
-        rows = pl.ds(pl.multiple_of(g * ROWS, ROWS), ROWS)
-        for k in range(2):
-            gate = dot(x_buf[rows, :], wg[k])
-            up = dot(x_buf[rows, :], wu[k])
-            hid = (gate / (1.0 + jnp.exp(-gate)) * up).astype(bf16)
-            h_buf[g * 2, :, k * F : (k + 1) * F] = hid[: ROWS // 2]
-            h_buf[g * 2 + 1, :, k * F : (k + 1) * F] = hid[ROWS // 2 :]
-        cp = pltpu.make_async_remote_copy(
+    def swap(g):
+        return pltpu.make_async_remote_copy(
             src_ref=h_buf.at[g * 2 + 1 - dm], dst_ref=h_recv.at[g],
             send_sem=h_send.at[g], recv_sem=h_rsem.at[g],
             device_id=(ep, x_hid), device_id_type=MESH,
         )
-        cp.start()
-
-        @pl.when(g == 0)
-        def _():
-            for late in w_copies[2:]:
-                late.wait()
-
-        cp.wait()
-
-        def down(q, _):
+
+    def hidden(g):
+        for side in (1 - dm, dm):
+            rows = pl.ds(pl.multiple_of((g * 2 + side) * (ROWS // 2), ROWS // 2), ROWS // 2)
+            for k in range(2):
+                gate = dot(x_buf[rows, :], wg[k])
+                up = dot(x_buf[rows, :], wu[k])
+                h_buf[g * 2 + side, :, k * F : (k + 1) * F] = (
+                    gate / (1.0 + jnp.exp(-gate)) * up
+                ).astype(bf16)
+            if side is not dm:
+                swap(g).start()
+
+    def down(g):
+        swap(g).wait()
+
+        def part(q, _):
             cols = pl.ds(pl.multiple_of(q * DQ, DQ), DQ)
             v = dot(h_buf[g * 2 + dm], wd[0 : 2 * F, cols])
             v = v + dot(h_recv[g], wd[2 * F : 4 * F, cols])
@@ -253,9 +267,10 @@
             )
             return 0
 
-        lax.fori_loop(0, 4, down, 0)
-
-        def give(q, _):
+        lax.fori_loop(0, 4, part, 0)
+
+    def give(g):
+        def one(q, _):
             j = q % 4
             to = (x + q // 4 + j) % 4
             src = ((g * 4 + to) * 4 + j) * HALF
@@ -272,7 +287,54 @@
 
             return 0
 
-        lax.fori_loop(0, 16, give, 0)
+        lax.fori_loop(0, 16, one, 0)
+
+    def expert(g, _):
+        @pl.when(g < 3)
+        def _():
+            arrived(x_buf, ROWS, x_recv.at[g])
+
+        @pl.when(g == 3)
+        def _():
+            arrived(x_buf, ROWS - HALF, x_recv.at[g])
+
+        hidden(g)
+
+        @pl.when(g == 1)
+        def _():
+            w_copies[2].wait()
+            send_weight(shard(2, 0, F // 2), shard(3, 0, F // 2), x_gate, 4)
+            w_copies[3].wait()
+            send_weight(shard(1, F // 2, F // 2), shard(3, F // 2, F // 2), x_hid, 5)
+
+        @pl.when(g == 2)
+        def _():
+            for k in (4, 5):
+                pltpu.make_async_remote_copy(
+                    src_ref=shard(1, 0, F // 2), dst_ref=shard(3, (k - 4) * (F // 2), F // 2),
+                    send_sem=w_send.at[k], recv_sem=w_recv.at[k],
+                    device_id=(ep, x_hid), device_id_type=MESH,
+                ).wait()
+            pl.semaphore_wait(ready, 3)
+
+            def early(i, _):
+                down(i)
+
+                @pl.when(i == 0)
+                def _():
+                    give(0)
+
+                return 0
+
+            lax.fori_loop(0, 3, early, 0)
+
+        @pl.when(g == 3)
+        def _():
+            give(1)
+            give(2)
+            down(3)
+            give(3)
+
         return 0
 
     lax.fori_loop(0, 4, expert, 0)
@@ -392,14 +454,15 @@
             dma((4,)),
             dma,
             dma((4,)),
-            dma((5,)),
-            dma((5,)),
+            dma((6,)),
+            dma((6,)),
             dma((4,)),
             dma((4,)),
             dma,
             dma((4,)),
             dma((3,)),
             dma((3,)),
+            pltpu.SemaphoreType.REGULAR,
         ],
         compiler_params=pltpu.CompilerParams(
             collective_id=0, has_side_effects=True, vmem_limit_bytes=62 * 2**20
@@ -408,8 +471,8 @@
     )(
         tokens,
         in_gain.reshape(1, D),
-        route_ids,
-        route_scores,
+        route_ids.T,
+        route_scores.T,
         gate_weight.reshape(D, F),
         up_weight.reshape(D, F),
         down_weight.reshape(F, D),

time: 165 us -> 137 us (0.83)
  Pallas kernels: 159 us -> 135 us
  local copies, waits for them, and re-layouts: 5.31 us -> 2.06 us
    pallas_call x1, Pallas kernels: 159 us -> 135 us  [per_device(): pl.pallas_call(kernel, out_shape=jax.ShapeDtypeStruct((T, DQ), bf16), in_...]
    unnamed x3 -> x1, local copies, waits for them, and re-layouts: 5.31 us -> 2.06 us
where the time goes in v2:
time: 137 us
  Pallas kernels  135 us (99%)
  local copies, waits for them, and re-layouts  2.06 us (2%)
    pallas_call x1, Pallas kernels, per_device(): pl.pallas_call(kernel, out_shape=jax.ShapeDtypeStruct((T, DQ), bf16), in_...  135 us

profile of v2, /device:TPU:1, one launch (start us, length us, event | category | flops | bytes accessed | tf_op | source)
XLA Modules:
  0.0 136.8 jit_solution(16921455988809760490)
XLA Ops:
  0.0 134.7 %routed_experts.1 = bf16[768,512]{1,0:T(8,128)(2,1)} custom-call(bf16[768,2048]{1,0:T(8,128)(2,1)} %tok_hbm.1, f32[1,2048]{1,0:T(1,128)} %bitcast.10, s32[2,768]{1,0:T(2,128)} %bitcast.11, f32[2,768]{1,0:T(2,128)} %bitcast.12, bf16[2048,256]{1,0:T(8,128)(2,1)} %bitcast.7, bf16[2048,256]{1,0:T(8,128)(2,1)} %bitcast.8, bf16[256,2048]{1,0:T(8,128)(2,1)} %bitcast.9, ...), custom_call_target="tpu_custom_call" | custom-call | tf_op jit(solution)/shard_map/routed_experts/pallas_call | solution.py:427
  134.7 2.1 %copy.10 = bf16[768,512]{1,0:T(8,128)(2,1)} copy(bf16[768,512]{1,0:T(8,128)(2,1)} %routed_experts.1) | data formatting | bytes 1572864

commit v3 on v2

--- a/solution.py
+++ b/solution.py
@@ -44,7 +44,6 @@
     x_gate = ((((x - c + 4) % 4) + 1 - 2 * (((x - c + 4) % 4) % 2)) + c) % 4
     x_hid = (xs + 1 - 2 * member + c + 3) % 4
     x_far = (x + 2) % 4
-    dm = (c + member) % 2
 
     def source_of(g, j, dc, sign):
         dy = (j + g + 1) % 4
@@ -56,10 +55,21 @@
     tok_copy.start()
     wg_copy = pltpu.make_async_copy(wg_hbm, wg.at[0], local_sem.at[1])
     wu_copy = pltpu.make_async_copy(wu_hbm, wu.at[0], local_sem.at[2])
-    wd_copy = pltpu.make_async_copy(wd_hbm, wd.at[pl.ds(0, F), :], local_sem.at[3])
+
+    def features(k):
+        return pl.ds(pl.multiple_of(k * DQ, DQ), DQ)
+
+    def shard(k, part):
+        return wd.at[pl.ds(k * F, F), pl.ds(part * DQ, DQ)]
+
+    wd_copies = [
+        pltpu.make_async_copy(wd_hbm.at[:, features(k)], shard(0, q), local_sem.at[3 + q])
+        for q, k in enumerate((x, x_gate))
+    ]
     wg_copy.start()
     wu_copy.start()
-    wd_copy.start()
+    for cp in wd_copies:
+        cp.start()
 
     barrier = pltpu.get_barrier_semaphore()
 
@@ -200,17 +210,21 @@
         cp.start()
         return cp
 
-    def shard(k, lo=0, size=F):
-        return wd.at[pl.ds(k * F + lo, size), :]
-
     pack(0, 0)
     pl.semaphore_wait(barrier, 34)
     w_copies = [
         send_weight(wg_hbm, wg.at[1], x_gate, 0),
         send_weight(wu_hbm, wu.at[1], x_gate, 1),
-        send_weight(wd_hbm, shard(2), x_hid, 2),
-        send_weight(wd_hbm, shard(1), x_gate, 3),
     ]
+    for k, to, parts in (
+        (2, x_hid, (x_hid, x_far)), (3, x_far, (x_far, x_hid)), (1, x_gate, (x_gate, x))
+    ):
+        for q in range(2):
+            pltpu.make_async_remote_copy(
+                src_ref=wd_hbm.at[:, features(parts[q])], dst_ref=shard(k, q),
+                send_sem=w_send.at[2], recv_sem=w_recv.at[2],
+                device_id=(ep, to), device_id_type=MESH,
+            ).start()
     dispatch(0, 0)
     for d in range(1, 4):
         pl.semaphore_signal(
@@ -232,62 +246,63 @@
 
     wg_copy.wait()
     wu_copy.wait()
-    wd_copy.wait()
-    for cp in w_copies[:2]:
+    for cp in wd_copies:
         cp.wait()
-
-    def swap(g):
+    for cp in w_copies:
+        cp.wait()
+
+    def swap(k):
         return pltpu.make_async_remote_copy(
-            src_ref=h_buf.at[g * 2 + 1 - dm], dst_ref=h_recv.at[g],
-            send_sem=h_send.at[g], recv_sem=h_rsem.at[g],
+            src_ref=h_buf.at[k], dst_ref=h_recv.at[k],
+            send_sem=h_send.at[k], recv_sem=h_rsem.at[k],
             device_id=(ep, x_hid), device_id_type=MESH,
         )
 
+    def block(k):
+        return pl.ds(pl.multiple_of(k * (ROWS // 2), ROWS // 2), ROWS // 2)
+
     def hidden(g):
-        for side in (1 - dm, dm):
-            rows = pl.ds(pl.multiple_of((g * 2 + side) * (ROWS // 2), ROWS // 2), ROWS // 2)
-            for k in range(2):
-                gate = dot(x_buf[rows, :], wg[k])
-                up = dot(x_buf[rows, :], wu[k])
-                h_buf[g * 2 + side, :, k * F : (k + 1) * F] = (
+        def side(i, _):
+            k = g * 2 + i
+            for q in range(2):
+                gate = dot(x_buf[block(k), :], wg[q])
+                up = dot(x_buf[block(k), :], wu[q])
+                h_buf[k, :, q * F : (q + 1) * F] = (
                     gate / (1.0 + jnp.exp(-gate)) * up
                 ).astype(bf16)
-            if side is not dm:
-                swap(g).start()
-
-    def down(g):
-        swap(g).wait()
-
-        def part(q, _):
-            cols = pl.ds(pl.multiple_of(q * DQ, DQ), DQ)
-            v = dot(h_buf[g * 2 + dm], wd[0 : 2 * F, cols])
-            v = v + dot(h_recv[g], wd[2 * F : 4 * F, cols])
-            y_buf[pl.ds(pl.multiple_of((g * 4 + q) * ROWS // 2, ROWS // 2), ROWS // 2), :] = (
-                v.astype(bf16)
-            )
+            swap(k).start()
             return 0
 
-        lax.fori_loop(0, 4, part, 0)
-
-    def give(g):
-        def one(q, _):
-            j = q % 4
-            to = (x + q // 4 + j) % 4
-            src = ((g * 4 + to) * 4 + j) * HALF
-            dst = ((g * 8 + dm * 4 + j) * 2 + half) * HALF
-            mine = (g == 3) & (j == 0) & (dm == 0) & (to == x)
+        lax.fori_loop(0, 2, side, 0)
+
+    def down(k):
+        swap(k).wait()
+        for q in range(2):
+            cols = slice(q * DQ, (q + 1) * DQ)
+            v = dot(h_buf[k], wd[0 : 2 * F, cols])
+            v = v + dot(h_recv[k], wd[2 * F : 4 * F, cols])
+            y_buf[block(k * 2 + q), :] = v.astype(bf16)
+
+    def give(k):
+        def one(n, _):
+            g, side = k // 2, k % 2
+            j, q = n % 4, (n // 4 + n) % 2
+            src = ((k * 2 + q) * 4 + j) * HALF
+            dst = ((k * 4 + j) * 2 + half) * HALF
+            mine = (k == 6) & (j == 0) & (q == 0)
 
             @pl.when(jnp.logical_not(mine))
             def _():
                 pltpu.make_async_remote_copy(
                     src_ref=at_rows(y_buf, src, HALF), dst_ref=at_rows(r_buf, dst, HALF),
                     send_sem=y_send, recv_sem=r_recv.at[g],
-                    device_id=(source_of(g, j, dm, -1), to), device_id_type=MESH,
+                    device_id=(source_of(g, j, side, -1), x + q * (x_gate - x)),
+                    device_id_type=MESH,
                 ).start()
 
             return 0
 
-        lax.fori_loop(0, 16, one, 0)
+        lax.fori_loop(0, 8, one, 0)
 
     def expert(g, _):
         @pl.when(g < 3)
@@ -300,50 +315,38 @@
 
         hidden(g)
 
-        @pl.when(g == 1)
-        def _():
-            w_copies[2].wait()
-            send_weight(shard(2, 0, F // 2), shard(3, 0, F // 2), x_gate, 4)
-            w_copies[3].wait()
-            send_weight(shard(1, F // 2, F // 2), shard(3, F // 2, F // 2), x_hid, 5)
-
         @pl.when(g == 2)
         def _():
-            for k in (4, 5):
-                pltpu.make_async_remote_copy(
-                    src_ref=shard(1, 0, F // 2), dst_ref=shard(3, (k - 4) * (F // 2), F // 2),
-                    send_sem=w_send.at[k], recv_sem=w_recv.at[k],
-                    device_id=(ep, x_hid), device_id_type=MESH,
-                ).wait()
+            for sem in (w_send, w_recv):
+                part = wd.at[pl.ds(F, 3 * F), :]
+                pltpu.make_async_copy(part, part, sem.at[2]).wait()
             pl.semaphore_wait(ready, 3)
 
-            def early(i, _):
-                down(i)
-
-                @pl.when(i == 0)
+            def early(k, _):
+                down(k)
+
+                @pl.when(k < 2)
                 def _():
-                    give(0)
+                    give(k)
 
                 return 0
 
-            lax.fori_loop(0, 3, early, 0)
+            lax.fori_loop(0, 6, early, 0)
 
         @pl.when(g == 3)
         def _():
-            give(1)
-            give(2)
-            down(3)
-            give(3)
+            for k in range(2, 6):
+                give(k)
+            for k in range(6, 8):
+                down(k)
+                give(k)
 
         return 0
 
     lax.fori_loop(0, 4, expert, 0)
-
-    @pl.when(dm == 0)
-    def _():
-        src = pl.ds(pl.multiple_of((12 + x) * 4 * HALF, 16), HALF)
-        dst = pl.ds(pl.multiple_of((48 + half) * HALF, 16), HALF)
-        r_buf[dst, :] = y_buf[src, :]
+    r_buf[pl.ds(pl.multiple_of((48 + half) * HALF, 16), HALF), :] = y_buf[
+        12 * 4 * HALF : (12 * 4 + 1) * HALF, :
+    ]
 
     comb[...] = jnp.zeros_like(comb)
 
@@ -359,11 +362,11 @@
 
         lax.fori_loop(0, 6, weigh, 0)
 
-        @pl.when(jnp.logical_or(g < 3, dm == 1))
+        @pl.when(g < 3)
         def _():
             arrived(r_buf, 16 * HALF, r_recv.at[g])
 
-        @pl.when(jnp.logical_and(g == 3, dm == 0))
+        @pl.when(g == 3)
         def _():
             arrived(r_buf, 15 * HALF, r_recv.at[g])
 
@@ -409,13 +412,7 @@
 
     arrived(s_buf, 31 * HALF, s_send)
 
-    @pl.when(dm == 0)
-    def _():
-        arrived(y_buf, 63 * HALF, y_send)
-
-    @pl.when(dm == 1)
-    def _():
-        arrived(y_buf, 64 * HALF, y_send)
+    arrived(y_buf, 63 * HALF, y_send)
 
 
 def per_device(
@@ -435,9 +432,9 @@
             pltpu.VMEM((4 * ROWS, D), bf16),
             pltpu.VMEM((2, D, F), bf16),
             pltpu.VMEM((2, D, F), bf16),
-            pltpu.VMEM((4 * F, D), bf16),
+            pltpu.VMEM((4 * F, 2 * DQ), bf16),
             pltpu.VMEM((8, ROWS // 2, 2 * F), bf16),
-            pltpu.VMEM((4, ROWS // 2, 2 * F), bf16),
+            pltpu.VMEM((8, ROWS // 2, 2 * F), bf16),
             pltpu.VMEM((64 * HALF, DQ), bf16),
             pltpu.VMEM((64 * HALF, DQ), bf16),
             pltpu.VMEM((128, T), f32),
@@ -451,13 +448,13 @@
             pltpu.VMEM((T, DQ), f32),
             pltpu.VMEM((8, T), f32),
             pltpu.VMEM((3, 8, T), f32),
-            dma((4,)),
+            dma((5,)),
             dma,
             dma((4,)),
-            dma((6,)),
-            dma((6,)),
-            dma((4,)),
-            dma((4,)),
+            dma((3,)),
+            dma((3,)),
+            dma((8,)),
+            dma((8,)),
             dma,
             dma((4,)),
             dma((3,)),

time: 137 us -> 134 us (0.978); the launches traced: 137 us -> 131 us
  Pallas kernels: 135 us -> 129 us
    pallas_call x1, Pallas kernels: 135 us -> 129 us  [per_device(): pl.pallas_call(kernel, out_shape=jax.ShapeDtypeStruct((T, DQ), bf16), in_...]
where the time goes in v3:
time: 134 us; the launch traced here: 131 us
  Pallas kernels  129 us (96%)
  local copies, waits for them, and re-layouts  2.06 us (2%)
    pallas_call x1, Pallas kernels, per_device(): pl.pallas_call(kernel, out_shape=jax.ShapeDtypeStruct((T, DQ), bf16), in_...  129 us

profile of v3, /device:TPU:1, one launch (start us, length us, event | category | flops | bytes accessed | tf_op | source)
XLA Modules:
  0.0 131.3 jit_solution(2348708971408221350)
XLA Ops:
  0.0 129.3 %routed_experts.1 = bf16[768,512]{1,0:T(8,128)(2,1)} custom-call(bf16[768,2048]{1,0:T(8,128)(2,1)} %tok_hbm.1, f32[1,2048]{1,0:T(1,128)} %bitcast.10, s32[2,768]{1,0:T(2,128)} %bitcast.11, f32[2,768]{1,0:T(2,128)} %bitcast.12, bf16[2048,256]{1,0:T(8,128)(2,1)} %bitcast.7, bf16[2048,256]{1,0:T(8,128)(2,1)} %bitcast.8, bf16[256,2048]{1,0:T(8,128)(2,1)} %bitcast.9, ...), custom_call_target="tpu_custom_call" | custom-call | tf_op jit(solution)/shard_map/routed_experts/pallas_call | solution.py:424
  129.3 2.1 %copy.10 = bf16[768,512]{1,0:T(8,128)(2,1)} copy(bf16[768,512]{1,0:T(8,128)(2,1)} %routed_experts.1) | data formatting | bytes 1572864

commit v4 on v3

--- a/solution.py
+++ b/solution.py
@@ -14,6 +14,14 @@
 HALF = 48
 ROWS = 4 * 2 * HALF
 DQ = 512
+STEPS = (
+    (2, 2), (1, 2), (2, 1), (3, 2),
+    (2, 3), (1, 1), (1, 3), (3, 1),
+    (3, 3), (2, 0), (0, 2), (0, 1),
+    (1, 0), (0, 3), (3, 0), (0, 0),
+)
+FAR = 5
+OWN = 3 * 8 + 3
 f32 = jnp.float32
 bf16 = jnp.bfloat16
 
@@ -31,7 +39,7 @@
     out_ref,
     tok, s_buf, x_buf, wg, wu, wd, h_buf, h_recv, y_buf, r_buf,
     slot_t, onehot, sel, col0, col1, mix0, mix1, rowsum, comb, ns_buf, ns_recv,
-    local_sem, s_send, x_recv, w_send, w_recv, h_send, h_rsem, y_send, r_recv, n_send, n_recv, ready,
+    local_sem, s_send, x_recv, f_send, f_recv, w_send, w_recv, h_send, h_rsem, y_send, r_recv, n_send, n_recv, ready,
 ):
     ep = lax.axis_index("ep")
     x = lax.axis_index("tp")
@@ -45,10 +53,10 @@
     x_hid = (xs + 1 - 2 * member + c + 3) % 4
     x_far = (x + 2) % 4
 
-    def source_of(g, j, dc, sign):
-        dy = (j + g + 1) % 4
+    def peer(p, dc, sign):
+        dz, dy = STEPS[p]
         return (
-            ((z + sign * j + 4) % 4) * 8 + ((y + sign * dy + 4) % 4) * 2 + (c + dc) % 2
+            ((z + sign * dz + 4) % 4) * 8 + ((y + sign * dy + 4) % 4) * 2 + (c + dc) % 2
         )
 
     tok_copy = pltpu.make_async_copy(tok_hbm, tok, local_sem.at[0])
@@ -89,8 +97,12 @@
     dz_l = ((lanes >> 3) - z) & 3
     dy_l = (((lanes >> 1) & 3) - y) & 3
     dc_l = ((lanes & 1) - c) & 1
-    base = ((((dy_l - dz_l + 3) & 3) * 8 + dc_l * 4 + dz_l) * CAP).astype(f32)
-
+    base = dc_l * (4 * CAP)
+    for p, (dz, dy) in enumerate(STEPS):
+        base = base + jnp.where(
+            dz_l * 4 + dy_l == dz * 4 + dy, (p // 4 * 8 + p % 4) * CAP, 0
+        )
+    base = base.astype(f32)
     lanes_f = lanes.astype(f32)
 
     def column(row):
@@ -164,17 +176,17 @@
 
     lax.fori_loop(0, 12, normalize, 0)
 
-    def pack(g, _):
+    def pack(g):
         for q in range(8):
             dc, j = q // 4, q % 4
-            e = source_of(g, j, dc, 1)
+            e = peer(g * 4 + j, dc, 1)
             first = ((x - (c + dc) % 2 + 5) % 4) // 2 * HALF
             want = lax.broadcasted_iota(jnp.int32, (HALF, T), 0) + first
             row = slot_t[pl.ds(e, 1), :]
             sel[q * HALF : (q + 1) * HALF, :] = jnp.where(
                 row == want.astype(f32), 1.0, 0.0
             ).astype(bf16)
-        rows = pl.ds(pl.multiple_of(g * ROWS, ROWS), ROWS)
+        rows = slice(g * ROWS, (g + 1) * ROWS)
 
         def part(n, _):
             cols = pl.ds(pl.multiple_of(n * 512, 512), 512)
@@ -182,25 +194,32 @@
             return 0
 
         lax.fori_loop(0, 4, part, 0)
-        return 0
-
-    def dispatch(g, _):
-        def one(q, _):
-            k, dc, j = q // 8, (q // 4) % 2, q % 4
-
-            @pl.when(jnp.logical_or(g < 3, q % 8 > 0))
-            def _():
-                row = (g * 8 + q % 8) * HALF + k * 16
-                pltpu.make_async_remote_copy(
-                    src_ref=at_rows(s_buf, row, 16), dst_ref=at_rows(x_buf, row, 16),
-                    send_sem=s_send, recv_sem=x_recv.at[g],
-                    device_id=(source_of(g, j, dc, 1), x), device_id_type=MESH,
-                ).start()
+
+    far_parity = (x + c + 1) % 2
+
+    def dispatch(steps, sem):
+        def one(n, _):
+            k, dc = n // 2, n % 2
+            for p in steps:
+                if p == 15:
+                    go = dc > 0
+                elif p < FAR:
+                    go = far_parity == p % 2
+                else:
+                    go = dc >= 0
+
+                @pl.when(go)
+                def _():
+                    row = (p // 4 * 8 + dc * 4 + p % 4) * HALF + k * 16
+                    pltpu.make_async_remote_copy(
+                        src_ref=at_rows(s_buf, row, 16), dst_ref=at_rows(x_buf, row, 16),
+                        send_sem=s_send, recv_sem=x_recv.at[sem],
+                        device_id=(peer(p, dc, 1), x), device_id_type=MESH,
+                    ).start()
 
             return 0
 
-        lax.fori_loop(0, 24, one, 0)
-        return 0
+        lax.fori_loop(0, 6, one, 0)
 
     def send_weight(src, dst, to, sem):
         cp = pltpu.make_async_remote_copy(
@@ -210,7 +229,7 @@
         cp.start()
         return cp
 
-    pack(0, 0)
+    pack(0)
     pl.semaphore_wait(barrier, 34)
     w_copies = [
         send_weight(wg_hbm, wg.at[1], x_gate, 0),
@@ -225,24 +244,36 @@
                 send_sem=w_send.at[2], recv_sem=w_recv.at[2],
                 device_id=(ep, to), device_id_type=MESH,
             ).start()
-    dispatch(0, 0)
+    dispatch(range(4), 0)
     for d in range(1, 4):
         pl.semaphore_signal(
             ready, inc=1, device_id=(ep, (x + d) % 4), device_id_type=MESH
         )
-
-    def pack_and_send(g, _):
-        pack(g, 0)
-        dispatch(g, 0)
-        return 0
-
-    lax.fori_loop(1, 4, pack_and_send, 0)
-    own = slice(24 * HALF, 25 * HALF)
+    pack(1)
+    dispatch(range(4, FAR), 0)
+    dispatch(range(FAR, 8), 1)
+    pack(2)
+    dispatch(range(8, 12), 2)
+    pack(3)
+    dispatch(range(12, 16), 3)
+    own = slice(OWN * HALF, (OWN + 1) * HALF)
     x_buf[own, :] = s_buf[own, :]
 
     def arrived(ref, rows, sem):
         part = ref.at[pl.ds(0, rows), :]
         pltpu.make_async_copy(part, part, sem).wait()
+
+    def hand(p):
+        row = (p // 4 * 8 + (member + p) % 2 * 4 + p % 4) * HALF
+        return pltpu.make_async_remote_copy(
+            src_ref=at_rows(x_buf, row, HALF), dst_ref=at_rows(x_buf, row, HALF),
+            send_sem=f_send, recv_sem=f_recv,
+            device_id=(ep, x_hid), device_id_type=MESH,
+        )
+
+    arrived(x_buf, FAR * HALF, x_recv.at[0])
+    for p in range(FAR):
+        hand(p).start()
 
     wg_copy.wait()
     wu_copy.wait()
@@ -283,74 +314,60 @@
             v = v + dot(h_recv[k], wd[2 * F : 4 * F, cols])
             y_buf[block(k * 2 + q), :] = v.astype(bf16)
 
-    def give(k):
-        def one(n, _):
-            g, side = k // 2, k % 2
+    def give(g, side):
+        k = g * 2 + side
+        for n in range(8):
             j, q = n % 4, (n // 4 + n) % 2
             src = ((k * 2 + q) * 4 + j) * HALF
             dst = ((k * 4 + j) * 2 + half) * HALF
-            mine = (k == 6) & (j == 0) & (q == 0)
-
-            @pl.when(jnp.logical_not(mine))
-            def _():
+
+            def one():
                 pltpu.make_async_remote_copy(
                     src_ref=at_rows(y_buf, src, HALF), dst_ref=at_rows(r_buf, dst, HALF),
                     send_sem=y_send, recv_sem=r_recv.at[g],
-                    device_id=(source_of(g, j, side, -1), x + q * (x_gate - x)),
+                    device_id=(peer(g * 4 + j, side, -1), (x, x_gate)[q]),
                     device_id_type=MESH,
                 ).start()
 
+            if (g, j, q) == (3, 3, 0):
+                pl.when(side > 0)(one)
+            else:
+                one()
+
+    def finish_group(g):
+        def one(side, _):
+            down(g * 2 + side)
+            give(g, side)
             return 0
 
-        lax.fori_loop(0, 8, one, 0)
-
-    def expert(g, _):
-        @pl.when(g < 3)
-        def _():
-            arrived(x_buf, ROWS, x_recv.at[g])
-
-        @pl.when(g == 3)
-        def _():
-            arrived(x_buf, ROWS - HALF, x_recv.at[g])
-
-        hidden(g)
-
-        @pl.when(g == 2)
-        def _():
-            for sem in (w_send, w_recv):
-                part = wd.at[pl.ds(F, 3 * F), :]
-                pltpu.make_async_copy(part, part, sem.at[2]).wait()
-            pl.semaphore_wait(ready, 3)
-
-            def early(k, _):
-                down(k)
-
-                @pl.when(k < 2)
-                def _():
-                    give(k)
-
-                return 0
-
-            lax.fori_loop(0, 6, early, 0)
-
-        @pl.when(g == 3)
-        def _():
-            for k in range(2, 6):
-                give(k)
-            for k in range(6, 8):
-                down(k)
-                give(k)
-
-        return 0
-
-    lax.fori_loop(0, 4, expert, 0)
-    r_buf[pl.ds(pl.multiple_of((48 + half) * HALF, 16), HALF), :] = y_buf[
-        12 * 4 * HALF : (12 * 4 + 1) * HALF, :
+        lax.fori_loop(0, 2, one, 0)
+
+    arrived(x_buf, (8 - FAR) * 2 * HALF, x_recv.at[1])
+    for sem in (f_send, f_recv):
+        arrived(x_buf, FAR * HALF, sem)
+    hidden(1)
+    hidden(0)
+    for sem in (w_send, w_recv):
+        part = wd.at[pl.ds(F, 3 * F), :]
+        pltpu.make_async_copy(part, part, sem.at[2]).wait()
+    pl.semaphore_wait(ready, 3)
+    finish_group(1)
+    arrived(x_buf, ROWS, x_recv.at[2])
+    hidden(2)
+    finish_group(0)
+    arrived(x_buf, ROWS - HALF, x_recv.at[3])
+    hidden(3)
+    finish_group(2)
+    finish_group(3)
+    r_buf[pl.ds(pl.multiple_of((OWN * 2 + half) * HALF, 16), HALF), :] = y_buf[
+        (12 * 4 + 3) * HALF : (12 * 4 + 4) * HALF, :
     ]
 
     comb[...] = jnp.zeros_like(comb)
 
-    def combine(g, _):
+    def combine(i, _):
+        g = i + (1 - 2 * (i % 2)) * (1 - i // 2)
+
         def weigh(b, _):
             rows = pl.ds(pl.multiple_of(b * 128, 128), 128)
             for q in range(6):
@@ -410,7 +427,14 @@
 
     lax.fori_loop(0, 6, finish, 0)
 
-    arrived(s_buf, 31 * HALF, s_send)
+    @pl.when(far_parity == 0)
+    def _():
+        arrived(s_buf, 27 * HALF, s_send)
+
+    @pl.when(far_parity == 1)
+    def _():
+        arrived(s_buf, 25 * HALF, s_send)
+
 
     arrived(y_buf, 63 * HALF, y_send)
 
@@ -451,6 +475,8 @@
             dma((5,)),
             dma,
             dma((4,)),
+            dma,
+            dma,
             dma((3,)),
             dma((3,)),
             dma((8,)),

time: 134 us -> 127 us (0.948); the launches traced: 131 us -> 126 us
  Pallas kernels: 129 us -> 124 us
    pallas_call x1, Pallas kernels: 129 us -> 124 us  [per_device(): pl.pallas_call(kernel, out_shape=jax.ShapeDtypeStruct((T, DQ), bf16), in_...]
where the time goes in v4:
time: 127 us; the launch traced here: 126 us
  Pallas kernels  124 us (98%)
  local copies, waits for them, and re-layouts  2.06 us (2%)
    pallas_call x1, Pallas kernels, per_device(): pl.pallas_call(kernel, out_shape=jax.ShapeDtypeStruct((T, DQ), bf16), in_...  124 us

profile of v4, /device:TPU:1, one launch (start us, length us, event | category | flops | bytes accessed | tf_op | source)
XLA Modules:
  0.0 126.5 jit_solution(11370951179814392741)
XLA Ops:
  0.0 124.4 %routed_experts.1 = bf16[768,512]{1,0:T(8,128)(2,1)} custom-call(bf16[768,2048]{1,0:T(8,128)(2,1)} %tok_hbm.1, f32[1,2048]{1,0:T(1,128)} %bitcast.10, s32[2,768]{1,0:T(2,128)} %bitcast.11, f32[2,768]{1,0:T(2,128)} %bitcast.12, bf16[2048,256]{1,0:T(8,128)(2,1)} %bitcast.7, bf16[2048,256]{1,0:T(8,128)(2,1)} %bitcast.8, bf16[256,2048]{1,0:T(8,128)(2,1)} %bitcast.9, ...), custom_call_target="tpu_custom_call" | custom-call | tf_op jit(solution)/shard_map/routed_experts/pallas_call | solution.py:448
  124.4 2.1 %copy.10 = bf16[768,512]{1,0:T(8,128)(2,1)} copy(bf16[768,512]{1,0:T(8,128)(2,1)} %routed_experts.1) | data formatting | bytes 1572864

commit v5 on v4

--- a/solution.py
+++ b/solution.py
@@ -15,10 +15,10 @@
 ROWS = 4 * 2 * HALF
 DQ = 512
 STEPS = (
-    (2, 2), (1, 2), (2, 1), (3, 2),
-    (2, 3), (1, 1), (1, 3), (3, 1),
-    (3, 3), (2, 0), (0, 2), (0, 1),
-    (1, 0), (0, 3), (3, 0), (0, 0),
+    (2, 2), (1, 2), (2, 3), (2, 1),
+    (3, 2), (0, 1), (0, 3), (2, 0),
+    (1, 1), (3, 3), (0, 2), (1, 0),
+    (1, 3), (3, 1), (3, 0), (0, 0),
 )
 FAR = 5
 OWN = 3 * 8 + 3
@@ -197,7 +197,7 @@
 
     far_parity = (x + c + 1) % 2
 
-    def dispatch(steps, sem):
+    def dispatch(steps):
         def one(n, _):
             k, dc = n // 2, n % 2
             for p in steps:
@@ -213,7 +213,7 @@
                     row = (p // 4 * 8 + dc * 4 + p % 4) * HALF + k * 16
                     pltpu.make_async_remote_copy(
                         src_ref=at_rows(s_buf, row, 16), dst_ref=at_rows(x_buf, row, 16),
-                        send_sem=s_send, recv_sem=x_recv.at[sem],
+                        send_sem=s_send, recv_sem=x_recv.at[0 if p < FAR else p // 4],
                         device_id=(peer(p, dc, 1), x), device_id_type=MESH,
                     ).start()
 
@@ -235,33 +235,44 @@
         send_weight(wg_hbm, wg.at[1], x_gate, 0),
         send_weight(wu_hbm, wu.at[1], x_gate, 1),
     ]
-    for k, to, parts in (
-        (2, x_hid, (x_hid, x_far)), (3, x_far, (x_far, x_hid)), (1, x_gate, (x_gate, x))
-    ):
+    for k, to, parts in ((2, x_hid, (x_hid, x_far)), (1, x_gate, (x_gate, x))):
         for q in range(2):
             pltpu.make_async_remote_copy(
                 src_ref=wd_hbm.at[:, features(parts[q])], dst_ref=shard(k, q),
-                send_sem=w_send.at[2], recv_sem=w_recv.at[2],
+                send_sem=w_send.at[1 + k], recv_sem=w_recv.at[1 + k],
                 device_id=(ep, to), device_id_type=MESH,
             ).start()
-    dispatch(range(4), 0)
+    dispatch(range(4))
     for d in range(1, 4):
         pl.semaphore_signal(
             ready, inc=1, device_id=(ep, (x + d) % 4), device_id_type=MESH
         )
     pack(1)
-    dispatch(range(4, FAR), 0)
-    dispatch(range(FAR, 8), 1)
+    dispatch(range(4, 8))
     pack(2)
-    dispatch(range(8, 12), 2)
+    dispatch(range(8, 12))
     pack(3)
-    dispatch(range(12, 16), 3)
+    dispatch(range(12, 16))
     own = slice(OWN * HALF, (OWN + 1) * HALF)
     x_buf[own, :] = s_buf[own, :]
 
     def arrived(ref, rows, sem):
         part = ref.at[pl.ds(0, rows), :]
         pltpu.make_async_copy(part, part, sem).wait()
+
+    def shard_copied(k):
+        part = wd.at[pl.ds(k * F, F), :]
+        for sem in (w_send, w_recv):
+            pltpu.make_async_copy(part, part, sem.at[1 + k]).wait()
+
+    def relay():
+        shard_copied(2)
+        for q in range(2):
+            pltpu.make_async_remote_copy(
+                src_ref=shard(2, 1 - q), dst_ref=shard(3, q),
+                send_sem=w_send.at[4], recv_sem=w_recv.at[4],
+                device_id=(ep, x_gate), device_id_type=MESH,
+            ).start()
 
     def hand(p):
         row = (p // 4 * 8 + (member + p) % 2 * 4 + p % 4) * HALF
@@ -281,6 +292,7 @@
         cp.wait()
     for cp in w_copies:
         cp.wait()
+    relay()
 
     def swap(k):
         return pltpu.make_async_remote_copy(
@@ -347,9 +359,8 @@
         arrived(x_buf, FAR * HALF, sem)
     hidden(1)
     hidden(0)
-    for sem in (w_send, w_recv):
-        part = wd.at[pl.ds(F, 3 * F), :]
-        pltpu.make_async_copy(part, part, sem.at[2]).wait()
+    shard_copied(1)
+    shard_copied(3)
     pl.semaphore_wait(ready, 3)
     finish_group(1)
     arrived(x_buf, ROWS, x_recv.at[2])
@@ -477,8 +488,8 @@
             dma((4,)),
             dma,
             dma,
-            dma((3,)),
-            dma((3,)),
+            dma((5,)),
+            dma((5,)),
             dma((8,)),
             dma((8,)),
             dma,

time: 127 us -> 122 us (0.961)
  Pallas kernels: 124 us -> 119 us
    pallas_call x1, Pallas kernels: 124 us -> 119 us  [per_device(): pl.pallas_call(kernel, out_shape=jax.ShapeDtypeStruct((T, DQ), bf16), in_...]
where the time goes in v5:
time: 122 us
  Pallas kernels  119 us (98%)
  local copies, waits for them, and re-layouts  2.06 us (2%)
    pallas_call x1, Pallas kernels, per_device(): pl.pallas_call(kernel, out_shape=jax.ShapeDtypeStruct((T, DQ), bf16), in_...  119 us

profile of v5, /device:TPU:1, one launch (start us, length us, event | category | flops | bytes accessed | tf_op | source)
XLA Modules:
  0.0 121.6 jit_solution(9788017929270530163)
XLA Ops:
  0.0 119.5 %routed_experts.1 = bf16[768,512]{1,0:T(8,128)(2,1)} custom-call(bf16[768,2048]{1,0:T(8,128)(2,1)} %tok_hbm.1, f32[1,2048]{1,0:T(1,128)} %bitcast.10, s32[2,768]{1,0:T(2,128)} %bitcast.11, f32[2,768]{1,0:T(2,128)} %bitcast.12, bf16[2048,256]{1,0:T(8,128)(2,1)} %bitcast.7, bf16[2048,256]{1,0:T(8,128)(2,1)} %bitcast.8, bf16[256,2048]{1,0:T(8,128)(2,1)} %bitcast.9, ...), custom_call_target="tpu_custom_call" | custom-call | tf_op jit(solution)/shard_map/routed_experts/pallas_call | solution.py:459
  119.5 2.1 %copy.10 = bf16[768,512]{1,0:T(8,128)(2,1)} copy(bf16[768,512]{1,0:T(8,128)(2,1)} %routed_experts.1) | data formatting | bytes 1572864

commit v6 on v5

--- a/solution.py
+++ b/solution.py
@@ -15,8 +15,8 @@
 ROWS = 4 * 2 * HALF
 DQ = 512
 STEPS = (
-    (2, 2), (1, 2), (2, 3), (2, 1),
-    (3, 2), (0, 1), (0, 3), (2, 0),
+    (1, 2), (3, 2), (2, 1), (2, 3),
+    (2, 2), (0, 1), (0, 3), (2, 0),
     (1, 1), (3, 3), (0, 2), (1, 0),
     (1, 3), (3, 1), (3, 0), (0, 0),
 )
@@ -35,10 +35,11 @@
 
 
 def kernel(
-    tok_hbm, gain_ref, ids_ref, score_ref, wg_hbm, wu_hbm, wd_hbm, og_ref,
-    out_ref,
+    tok_hbm, gain_hbm, ids_hbm, score_hbm, wg_hbm, wu_hbm, wd_hbm,
+    comb,
+    gain_ref, ids_ref, score_ref,
     tok, s_buf, x_buf, wg, wu, wd, h_buf, h_recv, y_buf, r_buf,
-    slot_t, onehot, sel, col0, col1, mix0, mix1, rowsum, comb, ns_buf, ns_recv,
+    slot_t, onehot, sel, col0, col1, mix0, mix1, rowsum, ns_buf, ns_recv,
     local_sem, s_send, x_recv, f_send, f_recv, w_send, w_recv, h_send, h_rsem, y_send, r_recv, n_send, n_recv, ready,
 ):
     ep = lax.axis_index("ep")
@@ -59,6 +60,14 @@
             ((z + sign * dz + 4) % 4) * 8 + ((y + sign * dy + 4) % 4) * 2 + (c + dc) % 2
         )
 
+    small_copies = [
+        pltpu.make_async_copy(a, b, local_sem.at[5 + i])
+        for i, (a, b) in enumerate(
+            ((ids_hbm, ids_ref), (score_hbm, score_ref), (gain_hbm, gain_ref))
+        )
+    ]
+    for cp in small_copies:
+        cp.start()
     tok_copy = pltpu.make_async_copy(tok_hbm, tok, local_sem.at[0])
     tok_copy.start()
     wg_copy = pltpu.make_async_copy(wg_hbm, wg.at[0], local_sem.at[1])
@@ -92,6 +101,9 @@
         pl.semaphore_signal(
             barrier, inc=1, device_id=(ep, (x + d) % 4), device_id_type=MESH
         )
+
+    for cp in small_copies:
+        cp.wait()
 
     lanes = lax.broadcasted_iota(jnp.int32, (128, 128), 1)
     dz_l = ((lanes >> 3) - z) & 3
@@ -433,7 +445,7 @@
         scale = jnp.broadcast_to(scale, (128, 128)).T
         for q in range(4):
             cols = slice(q * 128, (q + 1) * 128)
-            out_ref[rows, cols] = (comb[rows, cols] * scale * og_ref[:, cols]).astype(bf16)
+            comb[rows, cols] = comb[rows, cols] * scale
         return 0
 
     lax.fori_loop(0, 6, finish, 0)
@@ -456,12 +468,15 @@
     vmem = pl.BlockSpec(memory_space=pltpu.VMEM)
     hbm = pl.BlockSpec(memory_space=pl.ANY)
     dma = pltpu.SemaphoreType.DMA
-    return pl.pallas_call(
+    scaled = pl.pallas_call(
         kernel,
-        out_shape=jax.ShapeDtypeStruct((T, DQ), bf16),
-        in_specs=[hbm, vmem, vmem, vmem, hbm, hbm, hbm, vmem],
+        out_shape=jax.ShapeDtypeStruct((T, DQ), f32),
+        in_specs=[hbm] * 7,
         out_specs=vmem,
         scratch_shapes=[
+            pltpu.VMEM((1, D), f32),
+            pltpu.VMEM((2, T), jnp.int32),
+            pltpu.VMEM((2, T), f32),
             pltpu.VMEM((T, D), bf16),
             pltpu.VMEM((4 * ROWS, D), bf16),
             pltpu.VMEM((4 * ROWS, D), bf16),
@@ -480,10 +495,9 @@
             pltpu.VMEM((T, 128), f32),
             pltpu.VMEM((T, 128), f32),
             pltpu.VMEM((T, 128), f32),
-            pltpu.VMEM((T, DQ), f32),
             pltpu.VMEM((8, T), f32),
             pltpu.VMEM((3, 8, T), f32),
-            dma((5,)),
+            dma((8,)),
             dma,
             dma((4,)),
             dma,
@@ -510,8 +524,8 @@
         gate_weight.reshape(D, F),
         up_weight.reshape(D, F),
         down_weight.reshape(F, D),
-        out_gain.reshape(1, DQ),
     )
+    return (scaled * out_gain).astype(bf16)
 
 
 def solution(mesh):

time: 122 us -> 119 us (0.975)
  Pallas kernels: 119 us -> 116 us
  other arithmetic: 0 us -> 2.48 us
  local copies, waits for them, and re-layouts: 2.06 us -> 0.01 us
    pallas_call x1, Pallas kernels: 119 us -> 116 us  [per_device(): pl.pallas_call(kernel, out_shape=jax.ShapeDtypeStruct((T, DQ), f32), in_s...]
    convert_element_type x0 -> x1, other arithmetic: none -> 2.48 us  [per_device(): return (scaled * out_gain).astype(bf16)]
    unnamed x1 -> x2, local copies, waits for them, and re-layouts: 2.06 us -> 0.01 us
where the time goes in v6:
time: 119 us; the launch traced here: 118 us
  Pallas kernels  116 us (97%)
  other arithmetic  2.48 us (2%)
    pallas_call x1, Pallas kernels, per_device(): pl.pallas_call(kernel, out_shape=jax.ShapeDtypeStruct((T, DQ), f32), in_s...  116 us
    convert_element_type x1, other arithmetic, per_device(): return (scaled * out_gain).astype(bf16)  2.48 us

profile of v6, /device:TPU:1, one launch (start us, length us, event | category | flops | bytes accessed | tf_op | source)
XLA Modules:
  0.0 118.5 jit_solution(9222391923897779772)
XLA Ops:
  0.0 0.0 copy-start
  0.0 116.0 %routed_experts.1 = f32[768,512]{1,0:T(8,128)} custom-call(bf16[768,2048]{1,0:T(8,128)(2,1)} %tok_hbm.1, f32[1,2048]{1,0:T(1,128)} %bitcast.9, s32[2,768]{1,0:T(2,128)} %bitcast.10, f32[2,768]{1,0:T(2,128)} %bitcast.11, bf16[2048,256]{1,0:T(8,128)(2,1)} %bitcast.6, bf16[2048,256]{1,0:T(8,128)(2,1)} %bitcast.7, bf16[256,2048]{1,0:T(8,128)(2,1)} %bitcast.8), custom_call_target="tpu_custom_call" | custom-call | tf_op jit(solution)/shard_map/routed_experts/pallas_call | solution.py:471
  116.0 0.0 copy-done
  116.0 2.5 %multiply_convert_fusion = bf16[768,512]{1,0:T(8,128)(2,1)} fusion(f32[768,512]{1,0:T(8,128)} %routed_experts.1, f32[512]{0:T(512)S(1)} %copy-done), kind=kLoop, calls=%fused_computation | loop fusion | flops 786432 | bytes 2361344 | tf_op jit(solution)/shard_map/convert_element_type | solution.py:528
Async XLA Ops:
  0.0 116.0 %copy-start = (f32[512]{0:T(512)S(1)}, f32[512]{0:T(512)}, u32[]{:S(2)}) copy-start(f32[512]{0:T(512)} %param.15) | copy-start | bytes 6148

commit v7 on v6

--- a/solution.py
+++ b/solution.py
@@ -35,11 +35,11 @@
 
 
 def kernel(
-    tok_hbm, gain_hbm, ids_hbm, score_hbm, wg_hbm, wu_hbm, wd_hbm,
-    comb,
-    gain_ref, ids_ref, score_ref,
+    tok_hbm, gain_hbm, ids_hbm, score_hbm, wg_hbm, wu_hbm, wd_hbm, og_hbm,
+    out_ref,
+    gain_ref, ids_ref, score_ref, og_ref,
     tok, s_buf, x_buf, wg, wu, wd, h_buf, h_recv, y_buf, r_buf,
-    slot_t, onehot, sel, col0, col1, mix0, mix1, rowsum, ns_buf, ns_recv,
+    slot_t, onehot, sel, col0, col1, mix0, mix1, rowsum, comb, ns_buf, ns_recv,
     local_sem, s_send, x_recv, f_send, f_recv, w_send, w_recv, h_send, h_rsem, y_send, r_recv, n_send, n_recv, ready,
 ):
     ep = lax.axis_index("ep")
@@ -63,7 +63,7 @@
     small_copies = [
         pltpu.make_async_copy(a, b, local_sem.at[5 + i])
         for i, (a, b) in enumerate(
-            ((ids_hbm, ids_ref), (score_hbm, score_ref), (gain_hbm, gain_ref))
+            ((ids_hbm, ids_ref), (score_hbm, score_ref), (gain_hbm, gain_ref), (og_hbm, og_ref))
         )
     ]
     for cp in small_copies:
@@ -445,7 +445,7 @@
         scale = jnp.broadcast_to(scale, (128, 128)).T
         for q in range(4):
             cols = slice(q * 128, (q + 1) * 128)
-            comb[rows, cols] = comb[rows, cols] * scale
+            out_ref[rows, cols] = (comb[rows, cols] * scale * og_ref[:, cols]).astype(bf16)
         return 0
 
     lax.fori_loop(0, 6, finish, 0)
@@ -468,15 +468,16 @@
     vmem = pl.BlockSpec(memory_space=pltpu.VMEM)
     hbm = pl.BlockSpec(memory_space=pl.ANY)
     dma = pltpu.SemaphoreType.DMA
-    scaled = pl.pallas_call(
+    return pl.pallas_call(
         kernel,
-        out_shape=jax.ShapeDtypeStruct((T, DQ), f32),
-        in_specs=[hbm] * 7,
+        out_shape=jax.ShapeDtypeStruct((T, DQ), bf16),
+        in_specs=[hbm] * 8,
         out_specs=vmem,
         scratch_shapes=[
             pltpu.VMEM((1, D), f32),
             pltpu.VMEM((2, T), jnp.int32),
             pltpu.VMEM((2, T), f32),
+            pltpu.VMEM((1, DQ), f32),
             pltpu.VMEM((T, D), bf16),
             pltpu.VMEM((4 * ROWS, D), bf16),
             pltpu.VMEM((4 * ROWS, D), bf16),
@@ -495,9 +496,10 @@
             pltpu.VMEM((T, 128), f32),
             pltpu.VMEM((T, 128), f32),
             pltpu.VMEM((T, 128), f32),
+            pltpu.VMEM((T, DQ), f32),
             pltpu.VMEM((8, T), f32),
             pltpu.VMEM((3, 8, T), f32),
-            dma((8,)),
+            dma((9,)),
             dma,
             dma((4,)),
             dma,
@@ -524,8 +526,8 @@
         gate_weight.reshape(D, F),
         up_weight.reshape(D, F),
         down_weight.reshape(F, D),
+        out_gain.reshape(1, DQ),
     )
-    return (scaled * out_gain).astype(bf16)
 
 
 def solution(mesh):

time: 119 us -> 118 us (level)
  other arithmetic: 2.48 us -> 0 us
  local copies, waits for them, and re-layouts: 0.01 us -> 2.06 us
    convert_element_type x1 -> x0, other arithmetic: 2.48 us -> none  [per_device(): return (scaled * out_gain).astype(bf16)]
    unnamed x2 -> x1, local copies, waits for them, and re-layouts: 0.01 us -> 2.06 us
where the time goes in v7:
time: 118 us
  Pallas kernels  116 us (98%)
  local copies, waits for them, and re-layouts  2.06 us (2%)
    pallas_call x1, Pallas kernels, per_device(): pl.pallas_call(kernel, out_shape=jax.ShapeDtypeStruct((T, DQ), bf16), in_...  116 us

profile of v7, /device:TPU:1, one launch (start us, length us, event | category | flops | bytes accessed | tf_op | source)
XLA Modules:
  0.0 117.8 jit_solution(7966509086164360865)
XLA Ops:
  0.0 115.7 %routed_experts.1 = bf16[768,512]{1,0:T(8,128)(2,1)} custom-call(bf16[768,2048]{1,0:T(8,128)(2,1)} %tok_hbm.1, f32[1,2048]{1,0:T(1,128)} %bitcast.10, s32[2,768]{1,0:T(2,128)} %bitcast.11, f32[2,768]{1,0:T(2,128)} %bitcast.12, bf16[2048,256]{1,0:T(8,128)(2,1)} %bitcast.7, bf16[2048,256]{1,0:T(8,128)(2,1)} %bitcast.8, bf16[256,2048]{1,0:T(8,128)(2,1)} %bitcast.9, ...), custom_call_target="tpu_custom_call" | custom-call | tf_op jit(solution)/shard_map/routed_experts/pallas_call | solution.py:471
  115.7 2.1 %copy.10 = bf16[768,512]{1,0:T(8,128)(2,1)} copy(bf16[768,512]{1,0:T(8,128)(2,1)} %routed_experts.1) | data formatting | bytes 1572864

commit v8 on v7

--- a/solution.py
+++ b/solution.py
@@ -295,7 +295,7 @@
         )
 
     arrived(x_buf, FAR * HALF, x_recv.at[0])
-    for p in range(FAR):
+    for p in reversed(range(FAR)):
         hand(p).start()
 
     wg_copy.wait()

time: 118 us -> 118 us (level)
  no operation moved by 1% of the time
where the time goes in v8:
time: 118 us
  Pallas kernels  116 us (98%)
  local copies, waits for them, and re-layouts  2.06 us (2%)
    pallas_call x1, Pallas kernels, per_device(): pl.pallas_call(kernel, out_shape=jax.ShapeDtypeStruct((T, DQ), bf16), in_...  116 us

profile of v8, /device:TPU:1, one launch (start us, length us, event | category | flops | bytes accessed | tf_op | source)
XLA Modules:
  0.0 117.8 jit_solution(14787987222464199266)
XLA Ops:
  0.0 115.7 %routed_experts.1 = bf16[768,512]{1,0:T(8,128)(2,1)} custom-call(bf16[768,2048]{1,0:T(8,128)(2,1)} %tok_hbm.1, f32[1,2048]{1,0:T(1,128)} %bitcast.10, s32[2,768]{1,0:T(2,128)} %bitcast.11, f32[2,768]{1,0:T(2,128)} %bitcast.12, bf16[2048,256]{1,0:T(8,128)(2,1)} %bitcast.7, bf16[2048,256]{1,0:T(8,128)(2,1)} %bitcast.8, bf16[256,2048]{1,0:T(8,128)(2,1)} %bitcast.9, ...), custom_call_target="tpu_custom_call" | custom-call | tf_op jit(solution)/shard_map/routed_experts/pallas_call | solution.py:471
  115.7 2.1 %copy.10 = bf16[768,512]{1,0:T(8,128)(2,1)} copy(bf16[768,512]{1,0:T(8,128)(2,1)} %routed_experts.1) | data formatting | bytes 1572864
